TPU v7x, 32 devices: a whole 2x2x4 slice. The times are simulated.
32 devices in a mesh: ep: 8 (over z, core), tp: 4 (over y, x).
Axes of the slice: x: 2, y: 2, z: 4, core: 2. Of those that a mesh axis runs over, the one named last changes fastest.
Arguments:
- receptance: bfloat16 [2048, 2048], P('ep', 'tp'), may hold values from -6 to 6
- key_tensor: bfloat16 [2048, 2048], P('ep', 'tp'), may hold values from -6 to 6
- value_tensor: bfloat16 [2048, 2048], P('ep', 'tp'), may hold values from -6 to 6
- decay_data_input: bfloat16 [2048, 2048], P('ep', 'tp'), may hold values from -4 to 4
- correction_rate_input: bfloat16 [2048, 2048], P('ep', 'tp'), may hold values from -16 to 6
- mixer_output_gate: bfloat16 [2048, 2048], P('ep', 'tp'), may hold values from -6 to 6
- decay_channel_offset: float32 [2048], P('tp'), may hold values from -16 to -3
- head_norm_gain: float32 [2048], P('tp'), may hold values from 0.1 to 1.9
- self_key_weight: float32 [2048], P('tp'), may hold values from -2 to 2
- mixer_output_weight: bfloat16 [2048, 2048], P('tp'), may hold values from -0.125 to 0.125
- second_batch_rows: bfloat16 [1024, 2048], P('ep'), may hold values from -6 to 6
- routed_expert_index: int32 [1024, 4], P('ep'), may hold values from 0 to 7, all different within a row; in each aligned block of 128 rows (0 to 127, 128 to 255, ...) at most 96 rows name the same one
- routing_output_weight: float32 [1024, 4], P('ep'), may hold values from 0.1 to 1
- expert_norm_gain: float32 [2048], replicated, may hold values from 0.1 to 1.9
- expert_gate_weight: bfloat16 [8, 1024, 2048], P('ep', 'tp'), may hold values from -0.125 to 0.125
- expert_up_weight: bfloat16 [8, 1024, 2048], P('ep', 'tp'), may hold values from -0.125 to 0.125
- expert_down_weight: bfloat16 [8, 1024, 2048], P('ep', None, 'tp'), may hold values from -0.1875 to 0.1875
- common_expert_gate: bfloat16 [1024, 2048], P('tp'), may hold values from -0.125 to 0.125
- common_expert_up: bfloat16 [1024, 2048], P('tp'), may hold values from -0.125 to 0.125
- common_expert_down: bfloat16 [1024, 2048], P(None, 'tp'), may hold values from -0.1875 to 0.1875
Outputs:
- token_mixer_output: bfloat16 [2048, 2048], P(('ep', 'tp'))
- expert_out: bfloat16 [1024, 2048], P('ep', 'tp')
Inputs may be any that keep to these rules, and one draw needn't show every extreme that they name: `routed_expert_index`: each row names 4 different experts. Within the rows of one index of ep no expert is named by more than 96 rows, and that bound is met in some index's rows.
All inputs are finite; a program needn't handle non-finite values.
Results may differ from a plain program's by a relative error of at most 0.017.
Values may be sent and summed in bfloat16 or wider, within the bound.
A program may use at most 128 MiB of HBM per device.

v0:
```python
import math

import jax
import jax.numpy as jnp
from jax import lax
from jax.sharding import PartitionSpec as P

HEAD_CHANNELS = 64
SPAN = 64
HIGHEST = lax.Precision.HIGHEST
PRECISION = lax.Precision.HIGH
NORM_FLOOR = 1.0


def head_view(matrix):
    return matrix.astype(jnp.float32).reshape(matrix.shape[0], -1, HEAD_CHANNELS)


def complete_head_outputs(
    state_readout,
    receptance_rows,
    key_row_block,
    value_row_block,
    head_norm_gain,
    self_key_weight,
    mixer_output_gate,
):
    mean_part = jnp.mean(state_readout, axis=-1, keepdims=True)
    spread = jnp.mean(jnp.square(state_readout - mean_part), axis=-1, keepdims=True)
    normalized_rows = (state_readout - mean_part) * lax.rsqrt(spread + NORM_FLOOR)
    sequence_length = state_readout.shape[0]
    normalized_rows = normalized_rows.reshape(sequence_length, -1) * head_norm_gain
    self_key_term = (
        jnp.sum(
            receptance_rows * key_row_block * self_key_weight.reshape(-1, HEAD_CHANNELS),
            axis=-1,
            keepdims=True,
        )
        * value_row_block
    )
    mixer_result = (
        normalized_rows + self_key_term.reshape(sequence_length, -1)
    ) * mixer_output_gate.astype(jnp.float32)
    return mixer_result.astype(jnp.bfloat16)


def product(spec, left, right):
    return jnp.einsum(spec, left, right, precision=PRECISION, preferred_element_type=jnp.float32)


def lower_inverse(strict, size):
    at = jnp.arange(size)
    row, column = at[:, None], at[None, :]
    inverse = None
    block = 1
    while block < size:
        pair = (
            (row // (2 * block) == column // (2 * block))
            & (row // block % 2 == 1)
            & (column // block % 2 == 0)
        )
        below = jnp.where(pair, strict, 0.0)
        if inverse is None:
            inverse = jnp.eye(size, dtype=jnp.float32) - below
        else:
            inverse = inverse - product(
                "nhij,nhjk->nhik", product("nhij,nhjk->nhik", inverse, below), inverse
            )
        block *= 2
    return inverse


def mixer_part(
    receptance,
    key_tensor,
    value_tensor,
    decay_data_input,
    correction_rate_input,
    mixer_output_gate,
    decay_channel_offset,
    head_norm_gain,
    self_key_weight,
    mixer_output_weight,
    routed_pieces,
):
    row_count, width = receptance.shape
    head_count = width // HEAD_CHANNELS
    span = min(SPAN, row_count)
    block_count = row_count // span
    receptance_rows = head_view(receptance)
    key_row_block = head_view(key_tensor)
    value_row_block = head_view(value_tensor)

    def by_block(matrix):
        return (
            matrix.astype(jnp.float32)
            .reshape(block_count, span, head_count, HEAD_CHANNELS)
            .transpose(0, 2, 1, 3)
        )

    step_log = -math.exp(-0.5) * jax.nn.sigmoid(
        decay_channel_offset + decay_data_input.astype(jnp.float32)
    )
    at = jnp.arange(span)
    reach = (at[:, None] >= at[None, :]).astype(jnp.float32)
    step_log = by_block(step_log)
    total_log = jnp.einsum("ts,nhsd->nhtd", reach, step_log, precision=HIGHEST)
    recept, keys, values = by_block(receptance), by_block(key_tensor), by_block(value_tensor)
    units = keys * lax.rsqrt(jnp.sum(keys * keys, axis=-1, keepdims=True) + 1.0)
    corrections = units * jax.nn.sigmoid(by_block(correction_rate_input))
    grown = jnp.exp(-total_log)
    last_log = total_log[:, :, -1:, :]
    unit_in = units * jnp.exp(total_log - step_log)
    recept_in = recept * jnp.exp(total_log)
    tail = jnp.exp(last_log - total_log)
    scores = product(
        "nhtd,nhsd->nhts",
        jnp.concatenate([unit_in, recept_in], axis=2),
        jnp.concatenate([keys * grown, corrections * grown], axis=2),
    )
    before = at[:, None] > at[None, :]
    upto = at[:, None] >= at[None, :]
    unit_key = jnp.where(before, scores[:, :, :span, :span], 0.0)
    unit_fix = jnp.where(before, scores[:, :, :span, span:], 0.0)
    read_key = jnp.where(upto, scores[:, :, span:, :span], 0.0)
    read_fix = jnp.where(upto, scores[:, :, span:, span:], 0.0)
    inverse = lower_inverse(unit_fix, span)
    key_values = product(
        "nhts,nhsd->nhtd", jnp.concatenate([unit_key, read_key], axis=2), values
    )
    solved = product(
        "nhts,nhsd->nhtd",
        inverse,
        jnp.concatenate([unit_in, key_values[:, :, :span]], axis=3),
    )
    reads = jnp.concatenate([recept_in, key_values[:, :, span:]], axis=3) - product(
        "nhts,nhsd->nhtd", read_fix, solved
    )
    eye_head = jnp.eye(HEAD_CHANNELS, dtype=jnp.float32)
    fresh = product("nhtj,nhti->nhji", keys * tail, values)
    moves = jnp.concatenate(
        [eye_head * jnp.exp(last_log), fresh], axis=3
    ) - product("nhtj,nhti->nhji", corrections * tail, solved)
    whole = moves[0]
    for block in range(1, block_count):
        step = product("hij,hjk->hik", moves[block, :, :, :HEAD_CHANNELS], whole)
        whole = step + jnp.concatenate(
            [jnp.zeros_like(step[..., :HEAD_CHANNELS]), moves[block, :, :, HEAD_CHANNELS:]],
            axis=2,
        )
    whole, routed_pieces = lax.optimization_barrier((whole, routed_pieces))
    everything = lax.all_gather(whole.astype(jnp.bfloat16), "ep")
    mine = lax.axis_index("ep")
    state = jnp.zeros((head_count, HEAD_CHANNELS, HEAD_CHANNELS), jnp.float32)
    for k in range(lax.axis_size("ep") - 1):
        part = everything[k].astype(jnp.float32)
        new = product("hij,hjk->hik", part[..., :HEAD_CHANNELS], state)
        state = jnp.where(k < mine, new + part[..., HEAD_CHANNELS:], state)
    starts = [state]
    for block in range(block_count - 1):
        state = (
            product("hij,hjk->hik", moves[block, :, :, :HEAD_CHANNELS], state)
            + moves[block, :, :, HEAD_CHANNELS:]
        )
        starts.append(state)
    merged_output = reads[..., HEAD_CHANNELS:] + product(
        "nhtj,nhji->nhti", reads[..., :HEAD_CHANNELS], jnp.stack(starts)
    )
    merged_output = merged_output.transpose(0, 2, 1, 3).reshape(
        row_count, head_count, HEAD_CHANNELS
    )
    mixer_result = complete_head_outputs(
        merged_output,
        receptance_rows,
        key_row_block,
        value_row_block,
        head_norm_gain,
        self_key_weight,
        mixer_output_gate,
    )
    summed = lax.psum_scatter(
        jnp.dot(mixer_result, mixer_output_weight, preferred_element_type=jnp.float32).astype(
            jnp.bfloat16
        ),
        "tp",
        scatter_dimension=0,
        tiled=True,
    )
    return (summed, routed_pieces)


def activate(rows_in, gate_part, up_part):
    pre_gate = jnp.einsum("fd,rd->fr", gate_part, rows_in, preferred_element_type=jnp.float32)
    pre_up = jnp.einsum("fd,rd->fr", up_part, rows_in, preferred_element_type=jnp.float32)
    return (jax.nn.silu(pre_gate) * pre_up).astype(jnp.bfloat16)


def expert_entry(
    second_batch_rows,
    routed_expert_index,
    routing_output_weight,
    expert_norm_gain,
    common_expert_gate,
    common_expert_up,
):
    row_count, width = second_batch_rows.shape
    top_count = routed_expert_index.shape[1]
    peer_count = lax.axis_size("ep")
    slot_count = 3 * row_count * top_count // (2 * peer_count)
    widened = second_batch_rows.astype(jnp.float32)
    normalized_rows = (
        widened
        * lax.rsqrt(jnp.mean(widened * widened, axis=-1, keepdims=True) + NORM_FLOOR)
        * expert_norm_gain
    ).astype(jnp.bfloat16)
    flat_ids = routed_expert_index.reshape(-1)
    one_hot = (flat_ids[:, None] == jnp.arange(peer_count, dtype=jnp.int32)[None, :]).astype(
        jnp.int32
    )
    slot_rank = jnp.sum((jnp.cumsum(one_hot, axis=0) - 1) * one_hot, axis=1)
    target = flat_ids * slot_count + slot_rank
    owners = jnp.arange(row_count * top_count, dtype=jnp.int32) // top_count
    source_row = jnp.full((peer_count * slot_count,), row_count, jnp.int32).at[target].set(owners)
    padded = jnp.concatenate([normalized_rows, jnp.zeros((1, width), jnp.bfloat16)], axis=0)
    outgoing = jnp.take(padded, source_row, axis=0).reshape(peer_count, slot_count, width)
    shared_hidden = activate(normalized_rows, common_expert_gate, common_expert_up)
    piece_width = width // lax.axis_size("tp")
    own_slice = lax.dynamic_slice_in_dim(
        outgoing, lax.axis_index("tp") * piece_width, piece_width, 2
    )
    arrived = lax.all_to_all(own_slice, "ep", split_axis=0, concat_axis=0, tiled=True)
    return (arrived, shared_hidden, target)


def expert_exit(
    slots,
    pieces,
    shared_hidden,
    target,
    routing_output_weight,
    expert_gate_weight,
    expert_up_weight,
    expert_down_weight,
    common_expert_down,
):
    peer_count, slot_count = slots
    row_count, top_count = routing_output_weight.shape
    out_width = expert_down_weight.shape[2]
    gate_cols = expert_gate_weight[0]
    up_cols = expert_up_weight[0]
    pre_gate = jnp.einsum("fd,rd->fr", gate_cols, pieces, preferred_element_type=jnp.float32)
    pre_up = jnp.einsum("fd,rd->fr", up_cols, pieces, preferred_element_type=jnp.float32)
    routed_hidden = (jax.nn.silu(pre_gate) * pre_up).astype(jnp.bfloat16)
    both = lax.all_gather(
        jnp.concatenate([routed_hidden, shared_hidden], axis=1), "tp", axis=0, tiled=True
    )
    pieces = (both[:, : routed_hidden.shape[1]], both[:, routed_hidden.shape[1] :])
    routed_rows = expert_down_weight[0]
    routed_sum = jnp.einsum("fr,fd->rd", pieces[0], routed_rows, preferred_element_type=jnp.float32)
    shared_out = jnp.einsum(
        "fr,fd->rd", pieces[1], common_expert_down, preferred_element_type=jnp.float32
    )
    returned = lax.all_to_all(
        routed_sum.astype(jnp.bfloat16).reshape(peer_count, slot_count, out_width),
        "ep",
        split_axis=0,
        concat_axis=0,
        tiled=True,
    )
    picked = jnp.take(returned.reshape(-1, out_width), target, axis=0).reshape(
        row_count, top_count, out_width
    )
    merged_output = (
        jnp.sum(picked.astype(jnp.float32) * routing_output_weight[:, :, None], axis=1) + shared_out
    )
    return merged_output.astype(jnp.bfloat16)


def on_device(
    receptance,
    key_tensor,
    value_tensor,
    decay_data_input,
    correction_rate_input,
    mixer_output_gate,
    decay_channel_offset,
    head_norm_gain,
    self_key_weight,
    mixer_output_weight,
    second_batch_rows,
    routed_expert_index,
    routing_output_weight,
    expert_norm_gain,
    expert_gate_weight,
    expert_up_weight,
    expert_down_weight,
    common_expert_gate,
    common_expert_up,
    common_expert_down,
):
    arrived, shared_hidden, target = expert_entry(
        second_batch_rows,
        routed_expert_index,
        routing_output_weight,
        expert_norm_gain,
        common_expert_gate,
        common_expert_up,
    )
    arrived, receptance, key_tensor, value_tensor, decay_data_input, correction_rate_input = (
        lax.optimization_barrier(
            (
                arrived,
                receptance,
                key_tensor,
                value_tensor,
                decay_data_input,
                correction_rate_input,
            )
        )
    )
    flat_rows = arrived.reshape(-1, arrived.shape[2])
    pieces = lax.all_gather(flat_rows, "tp", axis=1, tiled=True)
    token_mixer_output, pieces = mixer_part(
        receptance,
        key_tensor,
        value_tensor,
        decay_data_input,
        correction_rate_input,
        mixer_output_gate,
        decay_channel_offset,
        head_norm_gain,
        self_key_weight,
        mixer_output_weight,
        pieces,
    )
    expert_out = expert_exit(
        arrived.shape[:2],
        pieces,
        shared_hidden,
        target,
        routing_output_weight,
        expert_gate_weight,
        expert_up_weight,
        expert_down_weight,
        common_expert_down,
    )
    return (token_mixer_output, expert_out)


def solution(mesh):
    in_specs = (
        P("ep", "tp"),
        P("ep", "tp"),
        P("ep", "tp"),
        P("ep", "tp"),
        P("ep", "tp"),
        P("ep", "tp"),
        P("tp"),
        P("tp"),
        P("tp"),
        P("tp", None),
        P("ep", None),
        P("ep", None),
        P("ep", None),
        P(),
        P("ep", "tp", None),
        P("ep", "tp", None),
        P("ep", None, "tp"),
        P("tp", None),
        P("tp", None),
        P(None, "tp"),
    )
    out_specs = (P(("ep", "tp"), None), P("ep", "tp"))
    return jax.shard_map(
        on_device, mesh=mesh, in_specs=in_specs, out_specs=out_specs, check_vma=False
    )
```

profile of v0, /device:TPU:0, one launch (start us, length us, event | category | flops | bytes accessed | tf_op | source)
XLA Modules:
  0.0 222.1 jit_solution(11237634688748817533)
XLA Ops:
  9.3 1.1 reduce-window.6
  10.8 2.4 %scatter_custom_fusion = s32[768]{0:T(1024)S(1)} fusion(s32[512]{0:T(512)S(1)} %bitcast.191, s32[512]{0:T(512)S(1)} %add_select_fusion, s32[]{:T(128)} %constant.328.clone.1), kind=kCustom, calls=%fused_computation.207 | custom fusion | bytes 3076 | tf_op jit(solution)/shard_map/scatter | solution.py:223
  13.3 1.2 fusion.31
  14.6 1.2 fusion.33
  15.9 4.3 %gather_fusion = bf16[768,2048]{1,0:T(8,128)(2,1)} fusion(bf16[129,2048]{1,0:T(8,128)(2,1)S(1)} %concatenate.33, s32[1024]{0:T(1024)S(1)} %pad_clamp_fusion.1), kind=kCustom, calls=%fused_computation | custom fusion | bytes 6294528 | tf_op jit(solution)/shard_map/jit(_take)/gather | solution.py:225
  20.2 2.3 %dynamic-slice_select_fusion = bf16[8,96,512]{2,1,0:T(8,128)(2,1)} fusion(bf16[8,96,2048]{2,1,0:T(8,128)(2,1)} %bitcast.177, s32[]{:T(128)S(6)} %select_n.364, pred[8,96]{1,0:T(8,128)(4,1)S(1)} %broadcast_in_dim.94), kind=kLoop, calls=%fused_computation.114 | loop fusion | flops 393216 | bytes 1573636 | tf_op jit(solution)/shard_map/jit(_take)/select_n | solution.py:225
  22.4 6.5 %all-to-all-start = ((bf16[8,96,512]{2,1,0:T(8,128)(2,1)}), bf16[8,96,512]{2,1,0:T(8,128)(2,1)}, u32[]{:S(2)}, u32[]{:S(2)}) async-start(bf16[8,96,512]{2,1,0:T(8,128)(2,1)} %dynamic-slice_select_fusion), calls=%async_computation | async-start | bytes 1572864 | tf_op jit(solution)/shard_map/all_to_all | solution.py:231
  29.9 2.4 %convolution_bitcast_fusion.4 = f32[256,128]{0,1:T(8,128)} fusion(bf16[128,2048]{1,0:T(8,128)(2,1)S(1)} %fusion.33, bf16[256,2048]{1,0:T(8,128)(2,1)} %param.37), kind=kOutput, calls=%fused_computation.60 | convolution fusion | flops 134217728 | bytes 1703936 | tf_op jit(solution)/shard_map/fd,rd->fr/dot_general | solution.py:193
  32.3 17.7 %all-to-all-done = bf16[8,96,512]{2,1,0:T(8,128)(2,1)} async-done(((bf16[8,96,512]{2,1,0:T(8,128)(2,1)}), bf16[8,96,512]{2,1,0:T(8,128)(2,1)}, u32[]{:S(2)}, u32[]{:S(2)}) %all-to-all-start) | async-done | bytes 786464 | tf_op jit(solution)/shard_map/all_to_all | solution.py:231
  51.0 2.1 add_divide_fusion
  53.1 1.2 reshape.842
  54.3 1.4 reshape.885
  55.7 1.6 copy.252
  57.7 2.3 %reshape.834 = f32[4,64,8,64]{3,2,1,0:T(8,128)} reshape(f32[256,512]{1,0:T(8,128)} %get-tuple-element.35) | data formatting | bytes 1048576 | tf_op jit(solution)/shard_map/reshape | solution.py:97
  59.9 2.4 %reshape.884 = f32[4,64,8,64]{1,0,3,2:T(4,128)} reshape(bf16[256,512]{0,1:T(8,128)(2,1)} %copy.246) | data formatting | bytes 786432 | tf_op jit(solution)/shard_map/reshape | solution.py:97
  62.3 2.6 %copy.248 = f32[4,64,8,64]{3,1,2,0:T(8,128)} copy(f32[4,64,8,64]{1,0,3,2:T(4,128)} %reshape.884) | data formatting | bytes 1048576 | tf_op jit(solution)/shard_map/reshape | solution.py:97
  64.8 5.0 %fusion.66 = (f32[4,8,64,64]{3,2,1,0:T(8,128)S(1)}, f32[4,8,64,64]{3,2,1,0:T(8,128)S(1)}, f32[4,8,64,64]{3,2,1,0:T(8,128)S(1)}, f32[4,8,64,64]{3,2,1,0:T(8,128)S(1)}, f32[4,8,64,64]{3,2,1,0:T(8,128)}) fusion(f32[4,64,8,64]{3,2,1,0:T(8,128)} %reshape.842, f32[4,8,64]{2,1,0:T(8,128)S(1)} %add_rsqrt_fusion.1, f32[4,64,8,64]{3,1,2,0:T(8,128)S(1)} %copy.252, ...), kind=kOutput, calls=%fused_computation.113 | convolution fusion | flops 101715968 | bytes 4726784 | tf_op jit(solution)/shard_map/ts,nhsd->nhtd/dot_general | solution.py:107
  69.8 2.3 %fusion.1 = f32[4,8,128,128]{3,2,1,0:T(8,128)S(1)} fusion(f32[4,8,64,64]{3,2,1,0:T(8,128)S(1)} %get-tuple-element.30, f32[4,8,64,64]{3,2,1,0:T(8,128)S(1)} %get-tuple-element.19, f32[4,8,64,64]{3,2,1,0:T(8,128)S(1)} %get-tuple-element.18, f32[4,8,64,64]{3,2,1,0:T(8,128)S(1)} %get-tuple-element.24), kind=kOutput, calls=%fused_computation.5 | convolution fusion | flops 201850880 | bytes 4194304 | tf_op jit(solution)/shard_map/nhtd,nhsd->nhts/dot_general | solution.py:48
  72.2 1.0 fusion.63
  73.2 1.9 convolution_subtract_fusion.4
  75.1 1.6 slice_select_fusion.4
  76.6 2.0 reshape.836
  79.9 2.6 %fusion.8 = f32[4,8,128,64]{3,2,1,0:T(8,128)S(1)} fusion(f32[4,8,64,64]{3,2,1,0:T(8,128)} %get-tuple-element.23, f32[4,8,64,64]{3,2,1,0:T(8,128)} %get-tuple-element.22, bf16[4,8,64,64]{3,1,2,0:T(8,128)(2,1)} %bitcast.178), kind=kOutput, calls=%fused_computation.12 | convolution fusion | flops 100925440 | bytes 2359296 | tf_op jit(solution)/shard_map/nhts,nhsd->nhtd/dot_general | solution.py:48
  88.8 1.2 fusion.128
  93.0 1.7 convolution_subtract_fusion.5
  96.7 25.7 %all-gather.5.cloned.1.call-done = bf16[768,2048]{1,0:T(8,128)(2,1)} async-done(((bf16[768,512]{1,0:T(8,128)(2,1)}), bf16[768,2048]{1,0:T(8,128)(2,1)}) %all-gather.5.cloned.1.call-update) | async-done | bytes 3145744 | tf_op jit(solution)/shard_map/all_gather | solution.py:322
  122.8 2.5 %fusion.30 = bf16[256,128]{0,1:T(8,128)(2,1)} fusion(bf16[128,2048]{1,0:T(8,128)(2,1)} %copy-done.14, bf16[256,2048]{1,0:T(8,128)(2,1)} %param.38, f32[256,128]{0,1:T(8,128)S(1)} %copy-done.19), kind=kOutput, calls=%fused_computation.61 | convolution fusion | flops 134414336 | bytes 1769472 | tf_op jit(solution)/shard_map/fd,rd->fr/dot_general | solution.py:194
  128.0 2.0 copy.274
  130.1 3.9 %convolution_subtract_fusion.6 = f32[4,8,64,128]{3,2,1,0:T(8,128)} fusion(f32[4,8,64,128]{3,2,1,0:T(8,128)} %copy-done.10, f32[4,8,128,128]{3,2,1,0:T(8,128)} %copy-done.1, f32[4,8,64,64]{3,2,1,0:T(8,128)} %get-tuple-element.20, f32[4,8,64,64]{3,2,1,0:T(8,128)S(1)} %copy-done.9, pred[64,64]{1,0:T(8,128)(4,1)S(1)} %iota_compare_fusion.2), kind=kOutput, calls=%fused_computation.27 | convolution fusion | flops 101318656 | bytes 4722688 | tf_op jit(solution)/shard_map/nhts,nhsd->nhtd/dot_general | solution.py:48
  134.0 1.0 convolution_bitcast_fusion.2
  135.2 1.0 fusion.19
  137.1 9.7 %all-gather.9.cloned.1.call-done = bf16[64,64,128]{2,1,0:T(8,128)(2,1)} async-done(((bf16[8,64,128]{2,1,0:T(8,128)(2,1)}), bf16[64,64,128]{2,1,0:T(8,128)(2,1)}) %all-gather.9.cloned.1.call-update) | async-done | bytes 1048592 | tf_op jit(solution)/shard_map/all_gather | solution.py:152
  146.9 1.2 fusion.27
  148.1 1.2 fusion.26
  149.3 1.2 fusion.25
  150.5 1.2 fusion.24
  151.7 1.3 fusion.23
  153.0 1.2 fusion.22
  154.2 1.2 fusion.21
  159.4 2.1 copy.273
  161.5 1.1 reshape.838
  162.9 3.2 %convolution_convert_fusion = bf16[256,2048]{1,0:T(8,128)(2,1)} fusion(bf16[512,2048]{1,0:T(8,128)(2,1)S(1)} %copy-done, bf16[256,512]{1,0:T(8,128)(2,1)} %param.25, f32[256,512]{1,0:T(8,128)} %copy.274, bf16[256,512]{1,0:T(8,128)(2,1)S(1)} %copy-done.16, f32[256,512]{1,0:T(8,128)} %copy.273, f32[256,512]{1,0:T(8,128)} %reshape.838, ...), kind=kOutput, calls=%fused_computation.4 | convolution fusion | flops 538574848 | bytes 5769216 | tf_op jit(solution)/shard_map/dot_general | solution.py:182
  166.2 15.0 %all-gather.7.cloned.1.call-done = bf16[1024,896]{0,1:T(8,128)(2,1)} async-done(((bf16[256,896]{0,1:T(8,128)(2,1)}), bf16[1024,896]{0,1:T(8,128)(2,1)}) %all-gather.7.cloned.1.call-update) | async-done | bytes 1835024 | tf_op jit(solution)/shard_map/all_gather | solution.py:254
  181.2 3.6 %fusion.14 = bf16[768,512]{1,0:T(8,128)(2,1)} fusion(bf16[1024,896]{0,1:T(8,128)(2,1)} %all-gather.7.cloned.1.call-done, bf16[1,1024,512]{2,1,0:T(8,128)(2,1)} %param.36), kind=kOutput, calls=%fused_computation.23 | convolution fusion | flops 805699584 | bytes 3407872 | tf_op jit(solution)/shard_map/fr,fd->rd/dot_general | solution.py:259
  184.8 4.6 %all-to-all-start.1 = ((bf16[8,96,512]{2,1,0:T(8,128)(2,1)}), bf16[8,96,512]{2,1,0:T(8,128)(2,1)S(1)}, u32[]{:S(2)}, u32[]{:S(2)}) async-start(bf16[8,96,512]{2,1,0:T(8,128)(2,1)} %bitcast.186), calls=%async_computation.2 | async-start | bytes 1572864 | tf_op jit(solution)/shard_map/all_to_all | solution.py:263
  189.8 20.5 %all-to-all-done.1 = bf16[8,96,512]{2,1,0:T(8,128)(2,1)S(1)} async-done(((bf16[8,96,512]{2,1,0:T(8,128)(2,1)}), bf16[8,96,512]{2,1,0:T(8,128)(2,1)S(1)}, u32[]{:S(2)}, u32[]{:S(2)}) %all-to-all-start.1) | async-done | bytes 786464 | tf_op jit(solution)/shard_map/all_to_all | solution.py:263
  210.3 2.0 gather_fusion.1
  213.3 2.3 %fusion.28 = bf16[128,512]{1,0:T(8,128)(2,1)} fusion(f32[128,512]{1,0:T(8,128)S(1)} %multiply_reduce_fusion, bf16[1024,512]{1,0:T(8,128)(2,1)} %param.39, bf16[1024,896]{0,1:T(8,128)(2,1)} %all-gather.7.cloned.1.call-done), kind=kOutput, calls=%fused_computation.57 | convolution fusion | flops 134348800 | bytes 1703936 | tf_op jit(solution)/shard_map/fr,fd->rd/dot_general | solution.py:260
  (151 shorter events, 26.8 us)
Async XLA Ops:
  7.2 155.7 %copy-start = (bf16[512,2048]{1,0:T(8,128)(2,1)S(1)}, bf16[512,2048]{1,0:T(8,128)(2,1)}, u32[]{:S(2)}) copy-start(bf16[512,2048]{1,0:T(8,128)(2,1)} %param.29) | copy-start | bytes 6291460
  15.8 14.1 %copy-start.14 = (bf16[128,2048]{1,0:T(8,128)(2,1)}, bf16[128,2048]{1,0:T(8,128)(2,1)S(1)}, u32[]{:S(2)}) copy-start(bf16[128,2048]{1,0:T(8,128)(2,1)S(1)} %fusion.33) | copy-start | bytes 1572868
  22.4 27.5 %copy-start.17 = (bf16[256,512]{1,0:T(8,128)(2,1)S(1)}, bf16[256,512]{1,0:T(8,128)(2,1)}, u32[]{:S(2)}) copy-start(bf16[256,512]{1,0:T(8,128)(2,1)} %param.21) | copy-start | bytes 786436
  22.4 27.7 %copy-start.18 = (bf16[256,512]{1,0:T(8,128)(2,1)S(1)}, bf16[256,512]{1,0:T(8,128)(2,1)}, u32[]{:S(2)}) copy-start(bf16[256,512]{1,0:T(8,128)(2,1)} %param.20) | copy-start | bytes 786436
  22.4 28.5 %copy-start.22 = (f32[512]{0:T(512)S(1)}, f32[512]{0:T(512)}, u32[]{:S(2)}) copy-start(f32[512]{0:T(512)} %param.26) | copy-start | bytes 6148
  22.4 27.5 %all-to-all-start = ((bf16[8,96,512]{2,1,0:T(8,128)(2,1)}), bf16[8,96,512]{2,1,0:T(8,128)(2,1)}, u32[]{:S(2)}, u32[]{:S(2)}) async-start(bf16[8,96,512]{2,1,0:T(8,128)(2,1)} %dynamic-slice_select_fusion), calls=%async_computation | async-start | bytes 1572864 | tf_op jit(solution)/shard_map/all_to_all | solution.py:231
  28.9 93.5 %all-gather.5.cloned.1.call-start = ((), (), s32[]{:S(2)}) async-start(), calls=%async_computation.3 | async-start | bytes 3932160 | tf_op jit(solution)/shard_map/all_gather | solution.py:322
  69.8 2.3 %copy-start.8 = (f32[4,8,64,64]{3,2,1,0:T(8,128)}, f32[4,8,64,64]{3,2,1,0:T(8,128)S(1)}, u32[]{:S(2)}) copy-start(f32[4,8,64,64]{3,2,1,0:T(8,128)S(1)} %get-tuple-element.30) | copy-start | bytes 1572868
  69.8 2.3 %copy-start.11 = (f32[4,8,64,64]{3,2,1,0:T(8,128)}, f32[4,8,64,64]{3,2,1,0:T(8,128)S(1)}, u32[]{:S(2)}) copy-start(f32[4,8,64,64]{3,2,1,0:T(8,128)S(1)} %get-tuple-element.19) | copy-start | bytes 1572868
  72.1 2.9 %copy-start.1 = (f32[4,8,128,128]{3,2,1,0:T(8,128)}, f32[4,8,128,128]{3,2,1,0:T(8,128)S(1)}, u32[]{:S(2)}) copy-start(f32[4,8,128,128]{3,2,1,0:T(8,128)S(1)} %fusion.1) | copy-start | bytes 6291460
  79.6 67.2 %all-gather.9.cloned.1.call-start = ((), (), s32[]{:S(2)}) async-start(), calls=%async_computation.6 | async-start | bytes 1179648 | tf_op jit(solution)/shard_map/all_gather | solution.py:152
  79.9 2.8 %copy-start.2 = (f32[4,8,128,128]{3,2,1,0:T(8,128)S(1)}, f32[4,8,128,128]{3,2,1,0:T(8,128)}, u32[]{:S(2)}) copy-start(f32[4,8,128,128]{3,2,1,0:T(8,128)} %copy-done.1) | copy-start | bytes 6291460
  79.9 2.8 %copy-start.6 = (f32[4,8,64,64]{3,2,1,0:T(8,128)S(1)}, f32[4,8,64,64]{3,2,1,0:T(8,128)}, u32[]{:S(2)}) copy-start(f32[4,8,64,64]{3,2,1,0:T(8,128)} %convolution_subtract_fusion.4) | copy-start | bytes 1572868
  88.8 1.6 copy-start.12
  90.4 1.2 copy-start.5
  90.4 1.4 copy-start.13
  91.3 3.5 %copy-start.10 = (f32[4,8,64,128]{3,2,1,0:T(8,128)}, f32[4,8,64,128]{3,2,1,0:T(8,128)S(1)}, u32[]{:S(2)}) copy-start(f32[4,8,64,128]{3,2,1,0:T(8,128)S(1)} %fusion.35) | copy-start | bytes 3145732
  91.3 1.7 copy-start.7
  94.8 1.0 copy-start.3
  94.8 28.0 %copy-start.19 = (f32[256,128]{0,1:T(8,128)S(1)}, f32[256,128]{0,1:T(8,128)}, u32[]{:S(2)}) copy-start(f32[256,128]{0,1:T(8,128)} %convolution_bitcast_fusion.4) | copy-start | bytes 393220
  122.5 7.6 %copy-start.9 = (f32[4,8,64,64]{3,2,1,0:T(8,128)S(1)}, f32[4,8,64,64]{3,2,1,0:T(8,128)}, u32[]{:S(2)}) copy-start(f32[4,8,64,64]{3,2,1,0:T(8,128)} %copy-done.8) | copy-start | bytes 1572868
  122.5 58.7 %all-gather.7.cloned.1.call-start = ((), (), s32[]{:S(2)}) async-start(), calls=%async_computation.5 | async-start | bytes 2293760 | tf_op jit(solution)/shard_map/all_gather | solution.py:254
  130.0 3.9 %copy-start.25 = (bf16[768,2048]{1,0:T(8,128)(2,1)S(1)}, bf16[768,2048]{1,0:T(8,128)(2,1)}, u32[]{:S(2)}) copy-start(bf16[768,2048]{1,0:T(8,128)(2,1)} %all-gather.5.cloned.1.call-done) | copy-start | bytes 9437188
  130.0 3.9 %copy-start.26 = (bf16[1,256,2048]{2,1,0:T(8,128)(2,1)S(1)}, bf16[1,256,2048]{2,1,0:T(8,128)(2,1)}, u32[]{:S(2)}) copy-start(bf16[1,256,2048]{2,1,0:T(8,128)(2,1)} %param.34) | copy-start | bytes 3145732
  134.0 1.2 copy-start.27
  135.2 1.0 copy-start.20
  137.1 18.3 %copy-start.4 = (f32[4,8,64,128]{3,2,1,0:T(8,128)S(1)}, f32[4,8,64,128]{3,2,1,0:T(8,128)}, u32[]{:S(2)}) copy-start(f32[4,8,64,128]{3,2,1,0:T(8,128)} %copy-done.3) | copy-start | bytes 3145732
  137.1 78.5 %reduce-scatter.2.cloned.1.call-start = ((), (), s32[]{:S(2)}) async-start(), calls=%async_computation.4 | async-start | bytes 1310720 | tf_op jit(solution)/shard_map/reduce_scatter | solution.py:181
  151.7 4.5 %copy-start.15 = (f32[4,8,64,128]{3,2,1,0:T(8,128)S(1)}, f32[4,8,64,128]{3,2,1,0:T(8,128)}, u32[]{:S(2)}) copy-start(f32[4,8,64,128]{3,2,1,0:T(8,128)} %convolution_subtract_fusion.6) | copy-start | bytes 3145732
  159.4 3.5 %copy-start.16 = (bf16[256,512]{1,0:T(8,128)(2,1)S(1)}, bf16[256,512]{1,0:T(8,128)(2,1)}, u32[]{:S(2)}) copy-start(bf16[256,512]{1,0:T(8,128)(2,1)} %param.22) | copy-start | bytes 786436
  159.4 3.5 %copy-start.23 = (f32[512]{0:T(512)S(1)}, f32[512]{0:T(512)}, u32[]{:S(2)}) copy-start(f32[512]{0:T(512)} %param.27) | copy-start | bytes 6148
  166.2 23.3 %copy-start.24 = (f32[128,4]{0,1:T(4,128)S(1)}, f32[128,4]{0,1:T(4,128)}, u32[]{:S(2)}) copy-start(f32[128,4]{0,1:T(4,128)} %param.32) | copy-start | bytes 6148
  166.2 23.5 %copy-start.21 = (s32[128,4]{0,1:T(4,128)S(1)}, s32[128,4]{0,1:T(4,128)}, u32[]{:S(2)}) copy-start(s32[128,4]{0,1:T(4,128)} %param.31) | copy-start | bytes 6148
  184.8 25.5 %all-to-all-start.1 = ((bf16[8,96,512]{2,1,0:T(8,128)(2,1)}), bf16[8,96,512]{2,1,0:T(8,128)(2,1)S(1)}, u32[]{:S(2)}, u32[]{:S(2)}) async-start(bf16[8,96,512]{2,1,0:T(8,128)(2,1)} %bitcast.186), calls=%async_computation.2 | async-start | bytes 1572864 | tf_op jit(solution)/shard_map/all_to_all | solution.py:263
Sparse Core Ops, SparseCore 0:
  79.7 42.6 all-gather.4
  124.6 22.2 all-gather.8
  148.7 32.4 all-gather.6
  184.5 27.9 reduce-scatter.1
where the time goes:
time: 223 us; the launch traced here: 222 us
  waiting for transfers between devices  88.7 us (40%)
  matrix products  53.8 us (24%)
  local copies, waits for them, and re-layouts  37.2 us (17%)
  other arithmetic  15.9 us (7%)
  between operations  14.6 us (7%)
  starting transfers between devices  11.9 us (5%)
    dot_general x30, matrix products, product(): jnp.einsum(spec, left, right, precision=PRECISION, preferred_element_type...  32.8 us
    all_gather x1, waiting for transfers between devices, on_device(): pieces = lax.all_gather(flat_rows, 'tp', axis=1, tiled=True)  25.7 us
    all_to_all x1, waiting for transfers between devices, expert_exit(): lax.all_to_all(routed_sum.astype(jnp.bfloat16).reshape(peer_count, slot_c...  20.5 us
    all_to_all x1, waiting for transfers between devices, expert_entry(): lax.all_to_all(own_slice, 'ep', split_axis=0, concat_axis=0, tiled=True)  17.7 us
    all_gather x1, waiting for transfers between devices, expert_exit(): lax.all_gather(jnp.concatenate([routed_hidden, shared_hidden], axis=1), '...  15 us
    reshape x6, local copies, waits for them, and re-layouts, by_block(): return matrix.astype(jnp.float32).reshape(block_count, span, head_count,...  12.2 us
    all_gather x1, waiting for transfers between devices, mixer_part(): everything = lax.all_gather(whole.astype(jnp.bfloat16), 'ep')  9.73 us
    all_to_all x1, starting transfers between devices, expert_entry(): lax.all_to_all(own_slice, 'ep', split_axis=0, concat_axis=0, tiled=True)  6.49 us
  transfers between devices with their start and end apart: 6, of which 5 were waited for; matrix products, arithmetic and copies ran while one was open for 27% of the time, Pallas kernels for 0%

commit v1 on v0

v1 whole, which is shorter than its diff:
```python
import functools
import math

import jax
import jax.numpy as jnp
from jax import lax
from jax.experimental import pallas as pl
from jax.experimental.pallas import tpu as pltpu
from jax.sharding import PartitionSpec as P

HEAD = 64
SPAN = 64
NORM_FLOOR = 1.0
F32 = jnp.float32
BF = jnp.bfloat16
MESH = pl.DeviceIdType.MESH
DIMS = {
    "nn": (((1,), (0,)), ((), ())),
    "nt": (((1,), (1,)), ((), ())),
    "tn": (((0,), (0,)), ((), ())),
}


def dot(a, b, form="nn"):
    return lax.dot_general(a, b, DIMS[form], preferred_element_type=F32)


def split(x):
    high = x.astype(BF)
    return high, (x - high.astype(F32)).astype(BF)


def spread(x, mask):
    copies = mask.shape[0] // x.shape[0]
    return (x if copies == 1 else jnp.concatenate([x] * copies, axis=0)) * mask


def per_head(a, b, mask, form="nn", fine=False):
    if not fine:
        return dot(a.astype(BF), spread(b.astype(BF), mask), form)
    a_high, a_low = split(a)
    b_high, b_low = split(b)
    rows = a.shape[0]
    both = dot(jnp.concatenate([a_high, a_low], axis=0), spread(b_high, mask), form)
    return both[:rows] + both[rows:] + dot(a_high, spread(b_low, mask), form)


def head_sum(x, mask):
    rows = x.shape[0]
    both = dot(jnp.concatenate(split(x), axis=0), mask)
    return both[:rows] + both[rows:]


def fold(full, mask32):
    full = full * mask32
    out = full[:HEAD]
    for i in range(1, full.shape[0] // HEAD):
        out = out + full[i * HEAD : (i + 1) * HEAD]
    return out


def iotas(rows, lanes):
    at = lax.broadcasted_iota(jnp.int32, (rows, lanes), 0)
    s = lax.broadcasted_iota(jnp.int32, (rows, lanes), 1) & (HEAD - 1)
    return at, s


def local_span(recept, keys, values, data, rate, offset, mask):
    group = recept.shape[1]
    at, s = iotas(SPAN, group)
    recept, keys, values = recept.astype(F32), keys.astype(F32), values.astype(F32)
    step = -math.exp(-0.5) * jax.nn.sigmoid(offset + data.astype(F32))
    row = lax.broadcasted_iota(jnp.int32, (SPAN, SPAN), 0)
    col = lax.broadcasted_iota(jnp.int32, (SPAN, SPAN), 1)
    reach = jnp.where(row >= col, 1.0, 0.0).astype(BF)
    step_high, step_low = split(step)
    total = dot(reach, step_high) + dot(reach, step_low)
    units = keys * lax.rsqrt(head_sum(keys * keys, mask) + 1.0)
    fixes = units * jax.nn.sigmoid(rate.astype(F32))
    last = total[SPAN - 1 : SPAN]
    grown = jnp.exp(-total)
    tail = jnp.exp(last - total)
    unit_in = units * jnp.exp(total - step)
    recept_in = recept * jnp.exp(total)
    zero = jnp.zeros((SPAN, group), F32)
    left = jnp.concatenate([unit_in, recept_in], axis=0)
    key_scores = per_head(left, keys * grown, mask, "nt")
    fix_scores = per_head(left, fixes * grown, mask, "nt")
    unit_key = jnp.where(at > s, key_scores[:SPAN], zero)
    unit_fix = jnp.where(at > s, fix_scores[:SPAN], zero)
    read_key = jnp.where(at >= s, key_scores[SPAN:], zero)
    read_fix = jnp.where(at >= s, fix_scores[SPAN:], zero)
    inverse = None
    for level in range(SPAN.bit_length() - 1):
        pair = (
            ((at >> (level + 1)) == (s >> (level + 1)))
            & (((at >> level) & 1) == 1)
            & (((s >> level) & 1) == 0)
        )
        below = jnp.where(pair, unit_fix, zero)
        if inverse is None:
            inverse = jnp.where(at == s, 1.0, 0.0) - below
        else:
            inverse = inverse - per_head(per_head(inverse, below, mask), inverse, mask)
    key_values = per_head(jnp.concatenate([unit_key, read_key], axis=0), values, mask)
    solved_state = per_head(inverse, unit_in, mask)
    solved_value = per_head(inverse, key_values[:SPAN], mask)
    read_state = recept_in - per_head(read_fix, solved_state, mask)
    read_value = key_values[SPAN:] - per_head(read_fix, solved_value, mask)
    key_tail = (keys * tail).astype(BF)
    fix_tail = (-fixes * tail).astype(BF)
    mask32 = mask.astype(F32)
    move = fold(dot(fix_tail, solved_state.astype(BF), "tn"), mask32)
    move = move + jnp.where(at == s, jnp.exp(last), zero)
    add = fold(
        dot(
            jnp.concatenate([key_tail, fix_tail], axis=0),
            jnp.concatenate([values.astype(BF), solved_value.astype(BF)], axis=0),
            "tn",
        ),
        mask32,
    )
    return read_state, read_value, move, add


def silu(v):
    return v / (1.0 + jnp.exp(-v))


def whole_kernel(
    sizes,
    recept_in, keys_in, values_in, data_in, rate_in, gate_in,
    offset_in, gain_in, self_in, out_weight_in,
    second_in, meta_in, norm_in,
    gate_w_in, up_w_in, down_w_in, common_gate_in, common_up_in, common_down_in,
    token_out, expert_out,
    mix, gate_v, out_w, second, rows, meta, gate_up, down, common, common_d,
    picks, hidden, shared, part, part_in, back, back_in, maps, reads, steps, mixed, mask_v,
    load_s, zs, zr, ms, mr, rs, rr, hs, hr, cs, cr, ps, pr, fs, fr, os, orr, bs, br, ws, wr,
):
    n_z, n_tp, top, cap = sizes
    e = lax.axis_index("ep")
    t = lax.axis_index("tp")
    z = e // 2
    c = e % 2
    positions, width = recept_in.shape
    group = min(256, width)
    groups = width // group
    spans = positions // SPAN
    row_count, model = second_in.shape
    piece = model // n_tp
    hid = common_gate_in.shape[0]

    partner = (e + 1 - 2 * c, t)

    def z_at(d):
        return (z + d) % n_z

    def z_dev(d):
        return (z_at(d) * 2 + c, t)

    def tp_dev(d):
        return (e, (t + d) % n_tp)

    def send(src, dst, ssem, rsem, dev):
        return pltpu.make_async_remote_copy(
            src_ref=src, dst_ref=dst, send_sem=ssem, recv_sem=rsem,
            device_id=dev, device_id_type=MESH,
        )

    def load(src, dst, k):
        return pltpu.make_async_copy(src, dst, load_s.at[k])

    loads = [
        load(second_in, second, 0),
        load(gate_w_in.at[0], gate_up.at[c, pl.ds(0, hid)], 1),
        load(up_w_in.at[0], gate_up.at[c, pl.ds(hid, hid)], 2),
        load(common_gate_in, common.at[pl.ds(0, hid)], 3),
        load(common_up_in, common.at[pl.ds(hid, hid)], 4),
        load(recept_in, mix.at[0], 5),
        load(keys_in, mix.at[1], 6),
        load(values_in, mix.at[2], 7),
        load(data_in, mix.at[3], 8),
        load(rate_in, mix.at[4], 9),
        load(gate_in, gate_v, 10),
        load(down_w_in.at[0], down.at[c], 11),
        load(out_weight_in, out_w, 12),
        load(common_down_in, common_d, 13),
    ]
    for copy in loads:
        copy.start()

    barrier = pltpu.get_barrier_semaphore()
    peers = [partner] + [z_dev(d) for d in range(1, n_z)] + [tp_dev(d) for d in range(1, n_tp)]
    for dev in peers:
        pl.semaphore_signal(barrier, inc=1, device_id=dev, device_id_type=MESH)

    loads[0].wait()
    wide = second[...].astype(F32)
    scale = lax.rsqrt(jnp.mean(wide * wide, axis=-1, keepdims=True) + NORM_FLOOR)
    for k in range(n_tp):
        lanes = pl.ds(k * piece, piece)
        rows[k, z] = (
            second[:, lanes].astype(F32) * scale * norm_in[:, lanes]
        ).astype(BF)
    meta[z] = meta_in[...]
    r_i = lax.broadcasted_iota(jnp.int32, (group, group), 0)
    c_i = lax.broadcasted_iota(jnp.int32, (group, group), 1)
    mask_v[...] = jnp.where((r_i >> 6) == (c_i >> 6), 1.0, 0.0).astype(BF)

    pl.semaphore_wait(barrier, len(peers))

    def rows_z(d):
        return send(rows.at[t, z], rows.at[t, z], zs.at[d], zr.at[d], z_dev(d))

    def rows_z_wait(d):
        w = z_at(n_z - d)
        return send(rows.at[t, w], rows.at[t, w], zs.at[d], zr.at[d], z_dev(d))

    def meta_z(d):
        return send(meta.at[z], meta.at[z], ms.at[d], mr.at[d], z_dev(d))

    def meta_z_wait(d):
        w = z_at(n_z - d)
        return send(meta.at[w], meta.at[w], ms.at[d], mr.at[d], z_dev(d))

    for d in range(1, n_z):
        rows_z(d).start()
    for d in range(1, n_z):
        meta_z(d).start()
    swap = [
        send(gate_w_in.at[0], gate_up.at[c, pl.ds(0, hid)], ws.at[0], wr.at[0], partner),
        send(up_w_in.at[0], gate_up.at[c, pl.ds(hid, hid)], ws.at[1], wr.at[1], partner),
        send(down_w_in.at[0], down.at[c], ws.at[2], wr.at[2], partner),
    ]
    swap_wait = [
        send(gate_w_in.at[0], gate_up.at[1 - c, pl.ds(0, hid)], ws.at[0], wr.at[0], partner),
        send(up_w_in.at[0], gate_up.at[1 - c, pl.ds(hid, hid)], ws.at[1], wr.at[1], partner),
        send(down_w_in.at[0], down.at[1 - c], ws.at[2], wr.at[2], partner),
    ]
    for copy in swap:
        copy.start()

    def both_dots(zz, weight):
        total = None
        for k in range(n_tp):
            term = dot(rows[k, zz], weight[:, k * piece : (k + 1) * piece], "nt")
            total = term if total is None else total + term
        return (silu(total[:, :hid]) * total[:, hid:]).astype(BF)

    def shared_to(d, slot):
        return send(shared.at[slot], shared.at[slot], cs.at[d], cr.at[d], tp_dev(d))

    loads[3].wait()
    loads[4].wait()
    shared[t] = both_dots(z, common)
    for d in range(1, n_tp):
        shared_to(d, t).start()

    def hidden_to(d, k, src):
        zz = z_at(d)
        return send(hidden.at[src, zz], hidden.at[src, zz], hs.at[d, k], hr.at[d, k], tp_dev(k))

    def routes(zz):
        cols = jnp.transpose(meta[zz])
        base = (z * 2).astype(F32)
        return cols, base

    def routed(d):
        zz = z_at(d)
        cols, base = routes(zz)
        lane = lax.broadcasted_iota(jnp.int32, (row_count, 128), 1).astype(F32) + base
        named = jnp.zeros((row_count, 128), F32)
        for k in range(top):
            named = named + jnp.where(cols[:, k : k + 1] == lane, 1.0, 0.0)
        row = lax.broadcasted_iota(jnp.int32, (row_count, row_count), 0)
        col = lax.broadcasted_iota(jnp.int32, (row_count, row_count), 1)
        rank = dot(jnp.where(row > col, 1.0, 0.0).astype(BF), named.astype(BF))
        slot = lax.broadcasted_iota(jnp.int32, (row_count, cap), 1).astype(F32)
        for x in range(2):
            pick = jnp.where(
                slot == rank[:, x : x + 1],
                jnp.broadcast_to(named[:, x : x + 1], (row_count, cap)),
                0.0,
            ).astype(BF)
            picks[zz, x] = pick
            units = both_dots(zz, gate_up[x])
            hidden[t, zz, pl.ds(x * cap, cap)] = dot(pick, units, "tn").astype(BF)
        for k in range(1, n_tp):
            hidden_to(d, k, t).start()

    loads[1].wait()
    loads[2].wait()
    swap_wait[0].wait_recv()
    swap_wait[1].wait_recv()
    routed(0)

    def relay_to(d, k, src):
        zz = z_at(d)
        return send(rows.at[src, zz], rows.at[src, zz], rs.at[d, k], rr.at[d, k], tp_dev(k))

    def relay(d):
        rows_z_wait(n_z - d).wait_recv()
        for k in range(1, n_tp):
            relay_to(d, k, t).start()

    for copy in loads[5:10]:
        copy.wait()
    per_step = -(-(n_z - 1) // spans)

    def span_step(b, carry):
        span = pl.ds(b * SPAN, SPAN)
        for g in range(groups):
            lanes = pl.ds(g * group, group)
            read_state, read_value, move, add = local_span(
                mix[0, span, lanes], mix[1, span, lanes], mix[2, span, lanes],
                mix[3, span, lanes], mix[4, span, lanes], offset_in[:, lanes], mask_v[...],
            )
            reads[0, span, lanes] = read_state
            reads[1, span, lanes] = read_value
            steps[0, b, :, lanes] = move
            steps[1, b, :, lanes] = add
        for i in range(per_step):
            d = b * per_step + i + 1

            @pl.when(d < n_z)
            def _():
                relay(d)

        return carry

    lax.fori_loop(0, spans, span_step, 0)

    for g in range(groups):
        lanes = pl.ds(g * group, group)
        mask = mask_v[...]
        move, add = steps[0, 0, :, lanes], steps[1, 0, :, lanes]
        for b in range(1, spans):
            here = steps[0, b, :, lanes]
            move, add = (
                per_head(here, move, mask, fine=True),
                per_head(here, add, mask, fine=True) + steps[1, b, :, lanes],
            )
        maps[z, c, :, lanes] = move.astype(BF)
        maps[z, c, :, pl.ds(width + g * group, group)] = add.astype(BF)

    def map_z(d):
        return send(maps.at[z, c], maps.at[z, c], ps.at[d], pr.at[d], z_dev(d))

    def map_z_wait(d):
        w = z_at(n_z - d)
        return send(maps.at[w, c], maps.at[w, c], ps.at[d], pr.at[d], z_dev(d))

    def map_on(d, core):
        w = z_at(n_z - d)
        return send(maps.at[w, core], maps.at[w, core], fs.at[d], fr.at[d], partner)

    for d in range(1, n_z):
        map_z(d).start()
    map_on(0, c).start()

    def routed_step(d, carry):
        meta_z_wait(n_z - d).wait_recv()
        for k in range(1, n_tp):
            relay_to(d, k, (t - k + n_tp) % n_tp).wait_recv()
        routed(d)
        return carry

    lax.fori_loop(1, n_z, routed_step, 0)

    for d in range(1, n_z):
        map_z_wait(d).wait_recv()
        map_on(d, c).start()
    for d in range(n_z):
        map_on(d, 1 - c).wait_recv()

    def prefix(i, state):
        both = maps[i // 2, i % 2]
        out = []
        for g in range(groups):
            lanes = slice(g * group, (g + 1) * group)
            after = slice(width + g * group, width + (g + 1) * group)
            out.append(
                per_head(both[:, lanes].astype(F32), state[:, lanes], mask_v[...], fine=True)
                + both[:, after].astype(F32)
            )
        return jnp.concatenate(out, axis=1) if groups > 1 else out[0]

    state = lax.fori_loop(0, e, prefix, jnp.zeros((HEAD, width), F32))

    loads[10].wait()

    def finish_step(b, state):
        span = pl.ds(b * SPAN, SPAN)
        following = []
        for g in range(groups):
            lanes = pl.ds(g * group, group)
            mask = mask_v[...]
            both = per_head(
                jnp.concatenate([reads[0, span, lanes], steps[0, b, :, lanes]], axis=0),
                state[:, g * group : (g + 1) * group],
                mask,
                fine=True,
            )
            following.append(both[SPAN:] + steps[1, b, :, lanes])
            read = reads[1, span, lanes] + both[:SPAN]
            recept, keys = mix[0, span, lanes].astype(F32), mix[1, span, lanes].astype(F32)
            sums = head_sum(
                jnp.concatenate([read, recept * keys * self_in[:, lanes]], axis=0), mask
            )
            apart = read - sums[:SPAN] * (1.0 / HEAD)
            spread_sum = head_sum(apart * apart, mask) * (1.0 / HEAD)
            normed = apart * lax.rsqrt(spread_sum + NORM_FLOOR) * gain_in[:, lanes]
            out = (normed + sums[SPAN:] * mix[2, span, lanes].astype(F32)) * gate_v[
                span, lanes
            ].astype(F32)
            mixed[span, lanes] = out.astype(BF)
        return jnp.concatenate(following, axis=1) if groups > 1 else following[0]

    lax.fori_loop(0, spans, finish_step, state)

    loads[12].wait()
    share = positions // n_tp
    wide_cols = min(512, model)

    def project(i, carry):
        lanes = pl.ds(pl.multiple_of(i * wide_cols, 128), wide_cols)
        got = dot(mixed[...], out_w[:, lanes]).astype(BF)
        for k in range(n_tp):
            part[k, :, lanes] = got[k * share : (k + 1) * share]
        return carry

    lax.fori_loop(0, model // wide_cols, project, 0)

    def part_to(d):
        return send(
            part.at[(t + d) % n_tp], part_in.at[d], os.at[d], orr.at[d], tp_dev(d)
        )

    for d in range(1, n_tp):
        part_to(d).start()

    loads[11].wait()
    swap_wait[2].wait_recv()

    def back_to(d):
        return send(back.at[z_at(d)], back_in.at[d], bs.at[d], br.at[d], z_dev(d))

    def routed_out(d):
        zz = z_at(d)
        cols, base = routes(zz)
        for k in range(1, n_tp):
            hidden_to(d, k, (t - k + n_tp) % n_tp).wait_recv()
        total = None
        for x in range(2):
            copies = None
            for k in range(n_tp):
                term = dot(
                    hidden[k, zz, pl.ds(x * cap, cap)], down[x, pl.ds(k * hid, hid)]
                )
                copies = term if copies is None else copies + term
            factor = jnp.zeros((row_count, 1), F32)
            for k in range(top):
                factor = factor + jnp.where(
                    cols[:, k : k + 1] == base + float(x), cols[:, top + k : top + k + 1], 0.0
                )
            term = dot(picks[zz, x], copies.astype(BF)) * factor
            total = term if total is None else total + term
        return total

    def back_step(d, carry):
        back[z_at(d)] = routed_out(d).astype(BF)
        back_to(d).start()
        return carry

    lax.fori_loop(1, n_z, back_step, 0)
    result = routed_out(0)

    loads[13].wait()
    for d in range(1, n_tp):
        shared_to(d, (t - d + n_tp) % n_tp).wait_recv()
    for k in range(n_tp):
        result = result + dot(shared[k], common_d[pl.ds(k * hid, hid)])

    for d in range(1, n_tp):
        part_to(d).wait_recv()
    summed = part[t].astype(F32)
    for d in range(1, n_tp):
        summed = summed + part_in[d].astype(F32)
    token_out[...] = summed.astype(BF)

    for d in range(1, n_z):
        back_to(d).wait_recv()
    for d in range(1, n_z):
        result = result + back_in[d].astype(F32)
    expert_out[...] = result.astype(BF)

    for copy in swap:
        copy.wait_send()
    for d in range(1, n_z):
        rows_z(d).wait_send()
        meta_z(d).wait_send()
        map_z(d).wait_send()
        back_to(d).wait_send()
    for d in range(n_z):
        map_on(d, c).wait_send()
        for k in range(1, n_tp):
            hidden_to(d, k, t).wait_send()
            if d:
                relay_to(d, k, t).wait_send()
    for k in range(1, n_tp):
        shared_to(k, t).wait_send()
        part_to(k).wait_send()


def on_device(n_ep, n_tp, *args):
    (
        receptance, key_tensor, value_tensor, decay_data_input, correction_rate_input,
        mixer_output_gate, decay_channel_offset, head_norm_gain, self_key_weight,
        mixer_output_weight, second_batch_rows, routed_expert_index, routing_output_weight,
        expert_norm_gain, expert_gate_weight, expert_up_weight, expert_down_weight,
        common_expert_gate, common_expert_up, common_expert_down,
    ) = args
    n_z = n_ep // 2
    positions, width = receptance.shape
    row_count, model = second_batch_rows.shape
    top = routed_expert_index.shape[1]
    cap = 3 * row_count * top // (2 * n_ep)
    cap = -(-cap // 16) * 16
    hid = common_expert_gate.shape[0]
    units = common_expert_down.shape[0]
    piece = model // n_tp
    group = min(256, width)
    spans = positions // SPAN
    meta = jnp.concatenate(
        [routed_expert_index.T.astype(F32), routing_output_weight.T], axis=0
    )
    any_spec = pl.BlockSpec(memory_space=pl.ANY)
    vmem = pl.BlockSpec(memory_space=pltpu.VMEM)
    dma = pltpu.SemaphoreType.DMA
    share = positions // n_tp
    return pl.pallas_call(
        functools.partial(whole_kernel, (n_z, n_tp, top, cap)),
        out_shape=(
            jax.ShapeDtypeStruct((share, model), BF),
            jax.ShapeDtypeStruct((row_count, piece), BF),
        ),
        in_specs=[any_spec] * 6 + [vmem] * 3 + [any_spec] + [any_spec, vmem, vmem] + [any_spec] * 6,
        out_specs=(vmem, vmem),
        scratch_shapes=[
            pltpu.VMEM((5, positions, width), BF),
            pltpu.VMEM((positions, width), BF),
            pltpu.VMEM((width, model), BF),
            pltpu.VMEM((row_count, model), BF),
            pltpu.VMEM((n_tp, n_z, row_count, piece), BF),
            pltpu.VMEM((n_z, 2 * top, row_count), F32),
            pltpu.VMEM((2, 2 * hid, model), BF),
            pltpu.VMEM((2, units, piece), BF),
            pltpu.VMEM((2 * hid, model), BF),
            pltpu.VMEM((units, piece), BF),
            pltpu.VMEM((n_z, 2, row_count, cap), BF),
            pltpu.VMEM((n_tp, n_z, 2 * cap, hid), BF),
            pltpu.VMEM((n_tp, row_count, hid), BF),
            pltpu.VMEM((n_tp, share, model), BF),
            pltpu.VMEM((n_tp, share, model), BF),
            pltpu.VMEM((n_z, row_count, piece), BF),
            pltpu.VMEM((n_z, row_count, piece), BF),
            pltpu.VMEM((n_z, 2, HEAD, 2 * width), BF),
            pltpu.VMEM((2, positions, width), F32),
            pltpu.VMEM((2, spans, HEAD, width), F32),
            pltpu.VMEM((positions, width), BF),
            pltpu.VMEM((group, group), BF),
            dma((14,)),
            dma((n_z,)), dma((n_z,)), dma((n_z,)), dma((n_z,)),
            dma((n_z, n_tp)), dma((n_z, n_tp)), dma((n_z, n_tp)), dma((n_z, n_tp)),
            dma((n_tp,)), dma((n_tp,)),
            dma((n_z,)), dma((n_z,)), dma((n_z,)), dma((n_z,)),
            dma((n_tp,)), dma((n_tp,)),
            dma((n_z,)), dma((n_z,)),
            dma((3,)), dma((3,)),
        ],
        compiler_params=pltpu.CompilerParams(
            collective_id=0, has_side_effects=True, vmem_limit_bytes=60 * 1024 * 1024
        ),
        name="mixer_and_experts",
    )(
        receptance, key_tensor, value_tensor, decay_data_input, correction_rate_input,
        mixer_output_gate, decay_channel_offset[None], head_norm_gain[None],
        self_key_weight[None], mixer_output_weight, second_batch_rows, meta,
        expert_norm_gain[None], expert_gate_weight, expert_up_weight, expert_down_weight,
        common_expert_gate, common_expert_up, common_expert_down,
    )


def solution(mesh):
    in_specs = (
        (P("ep", "tp"),) * 6
        + (P("tp"),) * 3
        + (P("tp", None),)
        + (P("ep", None),) * 3
        + (P(), P("ep", "tp", None), P("ep", "tp", None), P("ep", None, "tp"))
        + (P("tp", None), P("tp", None), P(None, "tp"))
    )
    out_specs = (P(("ep", "tp"), None), P("ep", "tp"))
    return jax.shard_map(
        functools.partial(on_device, mesh.shape["ep"], mesh.shape["tp"]),
        mesh=mesh, in_specs=in_specs, out_specs=out_specs, check_vma=False,
    )
```

time: 223 us -> 69.7 us (0.31)
  the two profiles are of different devices: /device:TPU:0 before, /device:TPU:1 now
where the time goes in v1:
time: 69.7 us; the launch traced here: 69.4 us
  Pallas kernels  63.5 us (91%)
  local copies, waits for them, and re-layouts  3.24 us (5%)
  other arithmetic  1.96 us (3%)
    pallas_call x1, Pallas kernels, on_device(): pl.pallas_call(functools.partial(whole_kernel, (n_z, n_tp, top, cap)), ou...  63.5 us
    unnamed x2, local copies, waits for them, and re-layouts  3.24 us

profile of v1, /device:TPU:1, one launch (start us, length us, event | category | flops | bytes accessed | tf_op | source)
XLA Modules:
  0.0 69.4 jit_solution(6141171380842479916)
XLA Ops:
  0.6 0.7 convert_bitcast_fusion
  1.3 1.3 %pad_maximum_fusion.meta_in = f32[8,128]{1,0:T(8,128)} fusion(f32[4,128]{1,0:T(4,128)} %bitcast.8, f32[4,128]{1,0:T(4,128)S(1)} %convert_bitcast_fusion), kind=kLoop, calls=%fused_computation | loop fusion | flops 1024 | bytes 8192 | tf_op jit(solution)/shard_map/concatenate | solution.py:535
  2.6 63.5 %mixer_and_experts.1 = (bf16[64,2048]{1,0:T(8,128)(2,1)}, bf16[128,512]{1,0:T(8,128)(2,1)}) custom-call(bf16[256,512]{1,0:T(8,128)(2,1)} %recept_in.1, bf16[256,512]{1,0:T(8,128)(2,1)} %keys_in.1, bf16[256,512]{1,0:T(8,128)(2,1)} %values_in.1, bf16[256,512]{1,0:T(8,128)(2,1)} %data_in.1, bf16[256,512]{1,0:T(8,128)(2,1)} %rate_in.1, ...), custom_call_target="tpu_custom_call" | custom-call | tf_op jit(solution)/shard_map/mixer_and_experts/pallas_call | solution.py:542
  66.1 1.7 %copy.24 = bf16[64,2048]{1,0:T(8,128)(2,1)} copy(bf16[64,2048]{1,0:T(8,128)(2,1)} %get-tuple-element.4) | data formatting | bytes 524288
  67.8 1.6 %copy.25 = bf16[128,512]{1,0:T(8,128)(2,1)} copy(bf16[128,512]{1,0:T(8,128)(2,1)} %get-tuple-element.5) | data formatting | bytes 262144

commit v2 on v1

v2 whole, which is shorter than its diff:
```python
import functools
import math

import jax
import jax.numpy as jnp
from jax import lax
from jax.experimental import pallas as pl
from jax.experimental.pallas import tpu as pltpu
from jax.sharding import PartitionSpec as P

HEAD = 64
SPAN = 64
SPANS_AT_ONCE = 2
NORM_FLOOR = 1.0
F32 = jnp.float32
BF = jnp.bfloat16
MESH = pl.DeviceIdType.MESH
DIMS = {
    "nn": (((1,), (0,)), ((), ())),
    "nt": (((1,), (1,)), ((), ())),
    "tn": (((0,), (0,)), ((), ())),
}


def dot(a, b, form="nn"):
    return lax.dot_general(a, b, DIMS[form], preferred_element_type=F32)


def split(x):
    high = x.astype(BF)
    return high, (x - high.astype(F32)).astype(BF)


def spread(x, mask):
    lanes = min(128, x.shape[1])
    tiles = x.shape[1] // lanes
    none = jnp.zeros((lanes, lanes), x.dtype)
    columns = []
    for j in range(tiles):
        piece = x[:, j * lanes : (j + 1) * lanes]
        block = jnp.concatenate([piece] * (lanes // HEAD), axis=0) * mask
        columns.append(jnp.concatenate([none] * j + [block] + [none] * (tiles - 1 - j), axis=0))
    return columns[0] if tiles == 1 else jnp.concatenate(columns, axis=1)


def per_head(a, b, mask, form="nn", fine=False):
    return per_heads([a], [b], mask, form, fine)[0]


def per_heads(lefts, rights, mask, form="nn", fine=False):
    if not fine:
        return [
            dot(a.astype(BF), spread(b.astype(BF), mask), form) for a, b in zip(lefts, rights)
        ]
    lefts, rights = [split(a) for a in lefts], [split(b) for b in rights]
    both = [
        dot(jnp.concatenate(a, axis=0), spread(b[0], mask), form) for a, b in zip(lefts, rights)
    ]
    rest = [dot(a[0], spread(b[1], mask), form) for a, b in zip(lefts, rights)]
    rows = lefts[0][0].shape[0]
    return [x[:rows] + x[rows:] + y for x, y in zip(both, rest)]


def head_sums(xs, ones):
    rows = xs[0].shape[0]
    both = [dot(jnp.concatenate(split(x), axis=0), ones) for x in xs]
    return [x[:rows] + x[rows:] for x in both]


def fold(full):
    lanes = min(128, full.shape[1])
    low = lax.broadcasted_iota(jnp.int32, (HEAD, lanes), 1) < HEAD
    out = []
    for j in range(full.shape[1] // lanes):
        block = full[:, j * lanes : (j + 1) * lanes]
        at = j * lanes
        out.append(
            jnp.where(low, block[at : at + HEAD], block[at + HEAD : at + 2 * HEAD])
            if lanes > HEAD
            else block[at : at + HEAD]
        )
    return out[0] if len(out) == 1 else jnp.concatenate(out, axis=1)


def iotas(rows, lanes):
    at = lax.broadcasted_iota(jnp.int32, (rows, lanes), 0)
    s = lax.broadcasted_iota(jnp.int32, (rows, lanes), 1) & (HEAD - 1)
    return at, s


def local_spans(problems, mask, ones):
    group = problems[0][0].shape[1]
    at, s = iotas(SPAN, group)
    zero = jnp.zeros((SPAN, group), F32)
    row = lax.broadcasted_iota(jnp.int32, (SPAN, SPAN), 0)
    col = lax.broadcasted_iota(jnp.int32, (SPAN, SPAN), 1)
    reach = jnp.where(row >= col, 1.0, 0.0).astype(BF)
    many = range(len(problems))
    recepts = [p[0].astype(F32) for p in problems]
    keys = [p[1].astype(F32) for p in problems]
    values = [p[2] for p in problems]
    step = [-math.exp(-0.5) * jax.nn.sigmoid(p[5] + p[3].astype(F32)) for p in problems]
    parts = [split(x) for x in step]
    high = [dot(reach, x[0]) for x in parts]
    low = [dot(reach, x[1]) for x in parts]
    total = [x + y for x, y in zip(high, low)]
    squares = head_sums([k * k for k in keys], ones)
    units = [k * lax.rsqrt(q + 1.0) for k, q in zip(keys, squares)]
    fixes = [u * jax.nn.sigmoid(p[4].astype(F32)) for u, p in zip(units, problems)]
    grown = [jnp.exp(-x) for x in total]
    unit_in = [units[i] * jnp.exp(total[i] - step[i]) for i in many]
    recept_in = [recepts[i] * jnp.exp(total[i]) for i in many]
    left = [jnp.concatenate([unit_in[i], recept_in[i]], axis=0) for i in many]
    fix_scores = per_heads(left, [fixes[i] * grown[i] for i in many], mask, "nt")
    key_scores = per_heads(left, [keys[i] * grown[i] for i in many], mask, "nt")
    unit_fix = [jnp.where(at > s, x[:SPAN], zero) for x in fix_scores]
    read_fix = [jnp.where(at >= s, x[SPAN:], zero) for x in fix_scores]
    both_key = [
        jnp.concatenate(
            [jnp.where(at > s, x[:SPAN], zero), jnp.where(at >= s, x[SPAN:], zero)], axis=0
        )
        for x in key_scores
    ]
    key_values = per_heads(both_key, values, mask)
    inverse = None
    for level in range(SPAN.bit_length() - 1):
        pair = (
            ((at >> (level + 1)) == (s >> (level + 1)))
            & (((at >> level) & 1) == 1)
            & (((s >> level) & 1) == 0)
        )
        below = [jnp.where(pair, x, zero) for x in unit_fix]
        if inverse is None:
            inverse = [jnp.where(at == s, 1.0, 0.0) - x for x in below]
        else:
            first = per_heads(inverse, below, mask)
            second = per_heads(first, inverse, mask)
            inverse = [x - y for x, y in zip(inverse, second)]
    solved_state = per_heads(inverse, unit_in, mask)
    solved_value = per_heads(inverse, [x[:SPAN] for x in key_values], mask)
    from_state = per_heads(read_fix, solved_state, mask)
    from_value = per_heads(read_fix, solved_value, mask)
    last = [x[SPAN - 1 : SPAN] for x in total]
    tail = [jnp.exp(last[i] - total[i]) for i in many]
    fix_tail = [(-fixes[i] * tail[i]).astype(BF) for i in many]
    key_tail = [(keys[i] * tail[i]).astype(BF) for i in many]
    moves = [dot(fix_tail[i], solved_state[i].astype(BF), "tn") for i in many]
    adds = [
        dot(
            jnp.concatenate([key_tail[i], fix_tail[i]], axis=0),
            jnp.concatenate([values[i], solved_value[i].astype(BF)], axis=0),
            "tn",
        )
        for i in many
    ]
    return [
        (
            recept_in[i] - from_state[i],
            key_values[i][SPAN:] - from_value[i],
            fold(moves[i]) + jnp.where(at == s, jnp.exp(last[i]), zero),
            fold(adds[i]),
        )
        for i in many
    ]


def silu(v):
    return v / (1.0 + jnp.exp(-v))


def whole_kernel(
    sizes,
    recept_in, keys_in, values_in, data_in, rate_in, gate_in,
    offset_in, gain_in, self_in, out_weight_in,
    second_in, ids_in, factor_in, norm_in,
    gate_w_in, up_w_in, down_w_in, common_gate_in, common_up_in, common_down_in,
    token_out, expert_out,
    mix, gate_v, out_w, second, rows, meta, gate_up, down, common, common_d,
    picks, hidden, shared, part, part_in, back, back_in, maps, reads, steps, mixed, mask_v,
    load_s, zs, zr, ms, mr, rs, rr, hs, hr, cs, cr, ps, pr, fs, fr, os, orr, bs, br, ws, wr,
):
    n_z, n_tp, top, cap = sizes
    e = lax.axis_index("ep")
    t = lax.axis_index("tp")
    z = e // 2
    c = e % 2
    positions, width = recept_in.shape
    group = min(256, width)
    groups = width // group
    lane_tile = min(128, group)
    spans = positions // SPAN
    row_count, model = second_in.shape
    piece = model // n_tp
    hid = common_gate_in.shape[0]

    partner = (e + 1 - 2 * c, t)

    def z_at(d):
        return (z + d) % n_z

    def z_dev(d):
        return (z_at(d) * 2 + c, t)

    def tp_dev(d):
        return (e, (t + d) % n_tp)

    def send(src, dst, ssem, rsem, dev):
        return pltpu.make_async_remote_copy(
            src_ref=src, dst_ref=dst, send_sem=ssem, recv_sem=rsem,
            device_id=dev, device_id_type=MESH,
        )

    def load(src, dst, k):
        return pltpu.make_async_copy(src, dst, load_s.at[k])

    loads = [
        load(second_in, second, 0),
        load(common_gate_in, common.at[pl.ds(0, hid)], 1),
        load(common_up_in, common.at[pl.ds(hid, hid)], 2),
        load(gate_w_in.at[0], gate_up.at[c, pl.ds(0, hid)], 3),
        load(up_w_in.at[0], gate_up.at[c, pl.ds(hid, hid)], 4),
        load(recept_in, mix.at[0], 5),
        load(keys_in, mix.at[1], 6),
        load(values_in, mix.at[2], 7),
        load(data_in, mix.at[3], 8),
        load(rate_in, mix.at[4], 9),
        load(gate_in, gate_v, 10),
        load(down_w_in.at[0], down.at[c], 11),
        load(out_weight_in, out_w, 12),
        load(common_down_in, common_d, 13),
    ]
    loads[0].start()

    barrier = pltpu.get_barrier_semaphore()
    peers = [partner] + [z_dev(d) for d in range(1, n_z)] + [tp_dev(d) for d in range(1, n_tp)]
    for dev in peers:
        pl.semaphore_signal(barrier, inc=1, device_id=dev, device_id_type=MESH)
    for copy in loads[1:5]:
        copy.start()

    r_i = lax.broadcasted_iota(jnp.int32, (group, group), 0)
    c_i = lax.broadcasted_iota(jnp.int32, (group, group), 1)
    mask_v[...] = jnp.where((r_i >> 6) == (c_i >> 6), 1.0, 0.0).astype(BF)
    meta[z] = jnp.concatenate([ids_in[...].astype(F32), factor_in[...]], axis=0)
    loads[0].wait()
    wide = second[...].astype(F32)
    scale = lax.rsqrt(jnp.mean(wide * wide, axis=-1, keepdims=True) + NORM_FLOOR)
    for k in range(n_tp):
        lanes = pl.ds(k * piece, piece)
        rows[k, z] = (
            second[:, lanes].astype(F32) * scale * norm_in[:, lanes]
        ).astype(BF)
    for copy in loads[5:]:
        copy.start()

    pl.semaphore_wait(barrier, len(peers))

    def rows_z(d):
        return send(rows.at[t, z], rows.at[t, z], zs.at[d], zr.at[d], z_dev(d))

    def rows_z_wait(d):
        w = z_at(n_z - d)
        return send(rows.at[t, w], rows.at[t, w], zs.at[d], zr.at[d], z_dev(d))

    def meta_z(d):
        return send(meta.at[z], meta.at[z], ms.at[d], mr.at[d], z_dev(d))

    def meta_z_wait(d):
        w = z_at(n_z - d)
        return send(meta.at[w], meta.at[w], ms.at[d], mr.at[d], z_dev(d))

    for d in range(1, n_z):
        rows_z(d).start()
    for d in range(1, n_z):
        meta_z(d).start()
    for copy in loads[3:5]:
        copy.wait()
    swap_up = send(gate_up.at[c], gate_up.at[c], ws.at[0], wr.at[0], partner)
    swap_up_in = send(gate_up.at[1 - c], gate_up.at[1 - c], ws.at[0], wr.at[0], partner)
    swap_down = send(down.at[c], down.at[c], ws.at[1], wr.at[1], partner)
    swap_down_in = send(down.at[1 - c], down.at[1 - c], ws.at[1], wr.at[1], partner)
    swap_up.start()

    square = n_tp == 4
    if square:
        x_t, y_t, far_t = t + 1 - 2 * (t % 2), (t + 2) % 4, 3 - t
        x_dev, y_dev = (e, x_t), (e, y_t)

    class Exchange:
        def __init__(self, whole, half, sem_s, sem_r):
            self.whole, self.half, self.sem_s, self.sem_r = whole, half, sem_s, sem_r

        def copy(self, ref, k, dev):
            return send(ref, ref, self.sem_s(k), self.sem_r(k), dev)

        def first(self):
            if square:
                return [self.copy(self.whole(t), 1, x_dev), self.copy(self.whole(t), 2, y_dev)]
            return [self.copy(self.whole(t), k, tp_dev(k)) for k in range(1, n_tp)]

        def second(self):
            if square:
                return [
                    self.copy(self.half(x_t, 0), 3, y_dev),
                    self.copy(self.half(y_t, 1), 0, x_dev),
                ]
            return []

        def start(self):
            for copy in self.first():
                copy.start()

        def forward(self):
            if square:
                ahead = [self.copy(self.whole(x_t), 1, x_dev), self.copy(self.whole(y_t), 2, y_dev)]
                for came, copy in zip(ahead, self.second()):
                    came.wait_recv()
                    copy.start()

        def finish(self):
            if square:
                self.copy(self.half(far_t, 0), 3, y_dev).wait_recv()
                self.copy(self.half(far_t, 1), 0, x_dev).wait_recv()
            else:
                for k in range(1, n_tp):
                    src = (t - k + n_tp) % n_tp
                    self.copy(self.whole(src), k, tp_dev(k)).wait_recv()

        def sent(self):
            for copy in self.first() + self.second():
                copy.wait_send()

    half_rows = row_count // 2
    shared_x = Exchange(
        lambda src: shared.at[src],
        lambda src, i: shared.at[src, pl.ds(i * half_rows, half_rows)],
        lambda k: cs.at[k], lambda k: cr.at[k],
    )

    def rows_x(d):
        zz = z_at(d)
        return Exchange(
            lambda src: rows.at[src, zz],
            lambda src, i: rows.at[src, zz, pl.ds(i * half_rows, half_rows)],
            lambda k: rs.at[d, k], lambda k: rr.at[d, k],
        )

    def hidden_x(d):
        zz = z_at(d)
        return Exchange(
            lambda src: hidden.at[src, zz],
            lambda src, i: hidden.at[src, zz, pl.ds(i * cap, cap)],
            lambda k: hs.at[d, k], lambda k: hr.at[d, k],
        )

    def each(low, high, step):
        if high - low <= 4:
            for d in range(low, high):
                step(d)
        else:
            def body(d, carry):
                step(d)
                return carry

            lax.fori_loop(low, high, body, 0)

    def both_dots(zz, weights):
        totals = [None] * len(weights)
        for i, weight in enumerate(weights):
            for k in range(n_tp):
                term = dot(rows[k, zz], weight[:, k * piece : (k + 1) * piece], "nt")
                totals[i] = term if totals[i] is None else totals[i] + term
        return [(silu(total[:, :hid]) * total[:, hid:]).astype(BF) for total in totals]

    for copy in loads[1:3]:
        copy.wait()
    shared[t] = both_dots(z, [common])[0]
    shared_x.start()

    def routes(zz):
        cols = jnp.transpose(meta[zz])
        base = (z * 2).astype(F32)
        return cols, base

    def routed(d):
        zz = z_at(d)
        cols, base = routes(zz)
        lane = lax.broadcasted_iota(jnp.int32, (row_count, 128), 1).astype(F32) + base
        named = jnp.zeros((row_count, 128), F32)
        for k in range(top):
            named = named + jnp.where(cols[:, k : k + 1] == lane, 1.0, 0.0)
        row = lax.broadcasted_iota(jnp.int32, (row_count, row_count), 0)
        col = lax.broadcasted_iota(jnp.int32, (row_count, row_count), 1)
        rank = dot(jnp.where(row > col, 1.0, 0.0).astype(BF), named.astype(BF))
        slot = lax.broadcasted_iota(jnp.int32, (row_count, cap), 1).astype(F32)
        units = both_dots(zz, [gate_up[0], gate_up[1]])
        chosen = [
            jnp.where(
                slot == rank[:, x : x + 1],
                jnp.broadcast_to(named[:, x : x + 1], (row_count, cap)),
                0.0,
            ).astype(BF)
            for x in range(2)
        ]
        packed = [dot(chosen[x], units[x], "tn").astype(BF) for x in range(2)]
        for x in range(2):
            picks[zz, x] = chosen[x]
            hidden[t, zz, pl.ds(x * cap, cap)] = packed[x]
        hidden_x(d).start()

    def relay(d):
        rows_z_wait(n_z - d).wait_recv()
        rows_x(d).start()

    stride = SPANS_AT_ONCE if spans % SPANS_AT_ONCE == 0 else 1

    def span_step(i):
        where = [
            (i * stride + j, pl.ds((i * stride + j) * SPAN, SPAN), pl.ds(g * group, group))
            for j in range(stride)
            for g in range(groups)
        ]
        found = local_spans(
            [
                tuple(mix[k, span, lanes] for k in range(5)) + (offset_in[:, lanes],)
                for _, span, lanes in where
            ],
            mask_v[:lane_tile, :lane_tile],
            mask_v[...],
        )
        for (b, span, lanes), (read_state, read_value, move, add) in zip(where, found):
            reads[0, span, lanes] = read_state
            reads[1, span, lanes] = read_value
            steps[0, b, :, lanes] = move
            steps[1, b, :, lanes] = add

    for copy in loads[5:10]:
        copy.wait()
    span_step(0)
    swap_up_in.wait_recv()
    routed(0)
    shared_x.forward()
    loads[11].wait()
    swap_down.start()
    each(1, min(3, n_z), relay)
    for i in range(1, spans // stride):
        span_step(i)
    hidden_x(0).forward()
    rows_x(1).forward()
    each(3, n_z, relay)

    tiles = [pl.ds(g * group, group) for g in range(groups)]
    mask = mask_v[:lane_tile, :lane_tile]
    now = [steps[0, 0, :, lanes] for lanes in tiles] + [steps[1, 0, :, lanes] for lanes in tiles]
    for b in range(1, spans):
        now = per_heads([steps[0, b, :, lanes] for lanes in tiles] * 2, now, mask, fine=True)
        for g, lanes in enumerate(tiles):
            now[groups + g] = now[groups + g] + steps[1, b, :, lanes]
    for k in range(2 * groups):
        maps[z, c, :, pl.ds(k * group, group)] = now[k].astype(BF)

    def map_z(d):
        return send(maps.at[z, c], maps.at[z, c], ps.at[d], pr.at[d], z_dev(d))

    def map_z_wait(d):
        w = z_at(n_z - d)
        return send(maps.at[w, c], maps.at[w, c], ps.at[d], pr.at[d], z_dev(d))

    def map_on(d, core):
        w = z_at(n_z - d)
        return send(maps.at[w, core], maps.at[w, core], fs.at[d], fr.at[d], partner)

    for d in range(1, n_z):
        map_z(d).start()
    map_on(0, c).start()

    def routed_step(d):
        meta_z_wait(n_z - d).wait_recv()
        if not isinstance(d, int):
            pl.when(d > 1)(lambda: rows_x(d).forward())
        elif d + 1 < n_z:
            rows_x(d + 1).forward()
        rows_x(d).finish()
        routed(d)
        if isinstance(d, int) and d > 1:
            hidden_x(d - 1).forward()

    each(1, n_z, routed_step)

    for d in range(1, n_z):
        map_z_wait(d).wait_recv()
        map_on(d, c).start()
    if n_z <= 5:
        hidden_x(n_z - 1).forward()
    for d in range(n_z):
        map_on(d, 1 - c).wait_recv()

    def prefix(i, state):
        both = maps[i // 2, i % 2]
        mask = mask_v[:lane_tile, :lane_tile]
        new = per_heads(
            [both[:, g * group : (g + 1) * group].astype(F32) for g in range(groups)],
            state, mask, fine=True,
        )
        return [
            new[g] + both[:, width + g * group : width + (g + 1) * group].astype(F32)
            for g in range(groups)
        ]

    state = lax.fori_loop(
        0, e, prefix, [jnp.zeros((HEAD, group), F32) for _ in range(groups)]
    )

    loads[10].wait()

    def finish_step(b, state):
        span = pl.ds(b * SPAN, SPAN)
        mask, ones = mask_v[:lane_tile, :lane_tile], mask_v[...]
        many = range(groups)
        recepts = [mix[0, span, lanes].astype(F32) for lanes in tiles]
        keys = [mix[1, span, lanes].astype(F32) for lanes in tiles]
        own = [recepts[g] * keys[g] * self_in[:, tiles[g]] for g in many]
        both = per_heads(
            [
                jnp.concatenate([reads[0, span, lanes], steps[0, b, :, lanes]], axis=0)
                for lanes in tiles
            ],
            state, mask, fine=True,
        )
        following = [both[g][SPAN:] + steps[1, b, :, tiles[g]] for g in many]
        read = [reads[1, span, tiles[g]] + both[g][:SPAN] for g in many]
        sums = head_sums([jnp.concatenate([read[g], own[g]], axis=0) for g in many], ones)
        apart = [read[g] - sums[g][:SPAN] * (1.0 / HEAD) for g in many]
        squares = head_sums([x * x for x in apart], ones)
        for g, lanes in enumerate(tiles):
            normed = (
                apart[g] * lax.rsqrt(squares[g] * (1.0 / HEAD) + NORM_FLOOR) * gain_in[:, lanes]
            )
            out = (normed + sums[g][SPAN:] * mix[2, span, lanes].astype(F32)) * gate_v[
                span, lanes
            ].astype(F32)
            mixed[span, lanes] = out.astype(BF)
        return following

    lax.fori_loop(0, spans, finish_step, state)

    loads[12].wait()
    share = positions // n_tp
    wide_cols = min(512, model)

    def project(i, carry):
        lanes = pl.ds(pl.multiple_of(i * wide_cols, 128), wide_cols)
        got = dot(mixed[...], out_w[:, lanes]).astype(BF)
        for k in range(n_tp):
            part[k, :, lanes] = got[k * share : (k + 1) * share]
        return carry

    lax.fori_loop(0, model // wide_cols, project, 0)

    def part_to(d):
        return send(
            part.at[(t + d) % n_tp], part_in.at[d], os.at[d], orr.at[d], tp_dev(d)
        )

    for d in range(1, n_tp):
        part_to(d).start()

    swap_down_in.wait_recv()

    def back_to(d):
        return send(back.at[z_at(d)], back_in.at[d], bs.at[d], br.at[d], z_dev(d))

    def routed_out(d):
        zz = z_at(d)
        cols, base = routes(zz)
        hidden_x(d).finish()
        copies = [None, None]
        for x in range(2):
            for k in range(n_tp):
                term = dot(
                    hidden[k, zz, pl.ds(x * cap, cap)], down[x, pl.ds(k * hid, hid)]
                )
                copies[x] = term if copies[x] is None else copies[x] + term
        terms = [dot(picks[zz, x], copies[x].astype(BF)) for x in range(2)]
        total = None
        for x in range(2):
            factor = jnp.zeros((row_count, 1), F32)
            for k in range(top):
                factor = factor + jnp.where(
                    cols[:, k : k + 1] == base + float(x), cols[:, top + k : top + k + 1], 0.0
                )
            term = terms[x] * factor
            total = term if total is None else total + term
        return total

    def back_step(d):
        if not isinstance(d, int):
            hidden_x(d).forward()
        back[z_at(d)] = routed_out(d).astype(BF)
        back_to(d).start()

    each(1, n_z, back_step)
    result = routed_out(0)

    loads[13].wait()
    shared_x.finish()
    for k in range(n_tp):
        result = result + dot(shared[k], common_d[pl.ds(k * hid, hid)])

    for d in range(1, n_tp):
        part_to(d).wait_recv()
    summed = part[t].astype(F32)
    for d in range(1, n_tp):
        summed = summed + part_in[d].astype(F32)
    token_out[...] = summed.astype(BF)

    for d in range(1, n_z):
        back_to(d).wait_recv()
    for d in range(1, n_z):
        result = result + back_in[d].astype(F32)
    expert_out[...] = result.astype(BF)

    swap_up.wait_send()
    swap_down.wait_send()
    for d in range(1, n_z):
        rows_z(d).wait_send()
        meta_z(d).wait_send()
        map_z(d).wait_send()
        back_to(d).wait_send()
        rows_x(d).sent()
    for d in range(n_z):
        map_on(d, c).wait_send()
        hidden_x(d).sent()
    shared_x.sent()
    for k in range(1, n_tp):
        part_to(k).wait_send()


def on_device(n_ep, n_tp, *args):
    (
        receptance, key_tensor, value_tensor, decay_data_input, correction_rate_input,
        mixer_output_gate, decay_channel_offset, head_norm_gain, self_key_weight,
        mixer_output_weight, second_batch_rows, routed_expert_index, routing_output_weight,
        expert_norm_gain, expert_gate_weight, expert_up_weight, expert_down_weight,
        common_expert_gate, common_expert_up, common_expert_down,
    ) = args
    n_z = n_ep // 2
    positions, width = receptance.shape
    row_count, model = second_batch_rows.shape
    top = routed_expert_index.shape[1]
    cap = 3 * row_count * top // (2 * n_ep)
    cap = -(-cap // 16) * 16
    hid = common_expert_gate.shape[0]
    units = common_expert_down.shape[0]
    piece = model // n_tp
    group = min(256, width)
    spans = positions // SPAN
    any_spec = pl.BlockSpec(memory_space=pl.ANY)
    vmem = pl.BlockSpec(memory_space=pltpu.VMEM)
    dma = pltpu.SemaphoreType.DMA
    share = positions // n_tp
    found = pl.pallas_call(
        functools.partial(whole_kernel, (n_z, n_tp, top, cap)),
        out_shape=(
            jax.ShapeDtypeStruct((share, model), BF),
            jax.ShapeDtypeStruct((row_count, piece), BF),
        ),
        in_specs=[any_spec] * 6 + [vmem] * 3 + [any_spec] + [any_spec, vmem, vmem, vmem] + [any_spec] * 6,
        out_specs=(vmem, vmem),
        scratch_shapes=[
            pltpu.VMEM((5, positions, width), BF),
            pltpu.VMEM((positions, width), BF),
            pltpu.VMEM((width, model), BF),
            pltpu.VMEM((row_count, model), BF),
            pltpu.VMEM((n_tp, n_z, row_count, piece), BF),
            pltpu.VMEM((n_z, 2 * top, row_count), F32),
            pltpu.VMEM((2, 2 * hid, model), BF),
            pltpu.VMEM((2, units, piece), BF),
            pltpu.VMEM((2 * hid, model), BF),
            pltpu.VMEM((units, piece), BF),
            pltpu.VMEM((n_z, 2, row_count, cap), BF),
            pltpu.VMEM((n_tp, n_z, 2 * cap, hid), BF),
            pltpu.VMEM((n_tp, row_count, hid), BF),
            pltpu.VMEM((n_tp, share, model), BF),
            pltpu.VMEM((n_tp, share, model), BF),
            pltpu.VMEM((n_z, row_count, piece), BF),
            pltpu.VMEM((n_z, row_count, piece), BF),
            pltpu.VMEM((n_z, 2, HEAD, 2 * width), BF),
            pltpu.VMEM((2, positions, width), F32),
            pltpu.VMEM((2, spans, HEAD, width), F32),
            pltpu.VMEM((positions, width), BF),
            pltpu.VMEM((group, group), BF),
            dma((14,)),
            dma((n_z,)), dma((n_z,)), dma((n_z,)), dma((n_z,)),
            dma((n_z, n_tp)), dma((n_z, n_tp)), dma((n_z, n_tp)), dma((n_z, n_tp)),
            dma((n_tp,)), dma((n_tp,)),
            dma((n_z,)), dma((n_z,)), dma((n_z,)), dma((n_z,)),
            dma((n_tp,)), dma((n_tp,)),
            dma((n_z,)), dma((n_z,)),
            dma((2,)), dma((2,)),
        ],
        compiler_params=pltpu.CompilerParams(
            collective_id=0, has_side_effects=True, vmem_limit_bytes=60 * 1024 * 1024
        ),
        name="mixer_and_experts",
    )(
        receptance, key_tensor, value_tensor, decay_data_input, correction_rate_input,
        mixer_output_gate, decay_channel_offset[None], head_norm_gain[None],
        self_key_weight[None], mixer_output_weight, second_batch_rows,
        routed_expert_index.T, routing_output_weight.T,
        expert_norm_gain[None], expert_gate_weight, expert_up_weight, expert_down_weight,
        common_expert_gate, common_expert_up, common_expert_down,
    )
    return pl.pallas_call(
        put_kernel,
        out_shape=tuple(jax.ShapeDtypeStruct(x.shape, x.dtype) for x in found),
        in_specs=[vmem] * 2,
        out_specs=(any_spec, any_spec),
        scratch_shapes=[dma((2,))],
        name="put_results",
    )(*found)


def put_kernel(token_in, expert_in, token_out, expert_out, sems):
    copies = [
        pltpu.make_async_copy(token_in, token_out, sems.at[0]),
        pltpu.make_async_copy(expert_in, expert_out, sems.at[1]),
    ]
    for copy in copies:
        copy.start()
    for copy in copies:
        copy.wait()


def solution(mesh):
    in_specs = (
        (P("ep", "tp"),) * 6
        + (P("tp"),) * 3
        + (P("tp", None),)
        + (P("ep", None),) * 3
        + (P(), P("ep", "tp", None), P("ep", "tp", None), P("ep", None, "tp"))
        + (P("tp", None), P("tp", None), P(None, "tp"))
    )
    out_specs = (P(("ep", "tp"), None), P("ep", "tp"))
    return jax.shard_map(
        functools.partial(on_device, mesh.shape["ep"], mesh.shape["tp"]),
        mesh=mesh, in_specs=in_specs, out_specs=out_specs, check_vma=False,
    )
```

time: 69.7 us -> 62.3 us (0.89)
  the two profiles are of different devices: /device:TPU:1 before, /device:TPU:0 now
where the time goes in v2:
time: 62.3 us; the launch traced here: 62.1 us
  Pallas kernels  61.3 us (98%)
  between operations  0.81 us (1%)
    pallas_call x1, Pallas kernels, on_device(): pl.pallas_call(functools.partial(whole_kernel, (n_z, n_tp, top, cap)), ou...  59.5 us
    pallas_call x1, Pallas kernels, on_device(): pl.pallas_call(put_kernel, out_shape=tuple((jax.ShapeDtypeStruct(x.shape,...  1.74 us

profile of v2, /device:TPU:0, one launch (start us, length us, event | category | flops | bytes accessed | tf_op | source)
XLA Modules:
  0.0 62.1 jit_solution(15289447503059419372)
XLA Ops:
  0.6 59.5 %mixer_and_experts.1 = (bf16[64,2048]{1,0:T(8,128)(2,1)}, bf16[128,512]{1,0:T(8,128)(2,1)}) custom-call(bf16[256,512]{1,0:T(8,128)(2,1)} %recept_in.1, bf16[256,512]{1,0:T(8,128)(2,1)} %keys_in.1, bf16[256,512]{1,0:T(8,128)(2,1)} %values_in.1, bf16[256,512]{1,0:T(8,128)(2,1)} %data_in.1, bf16[256,512]{1,0:T(8,128)(2,1)} %rate_in.1, ...), custom_call_target="tpu_custom_call" | custom-call | tf_op jit(solution)/shard_map/mixer_and_experts/pallas_call | solution.py:662
  60.2 1.7 %put_results.1 = (bf16[64,2048]{1,0:T(8,128)(2,1)}, bf16[128,512]{1,0:T(8,128)(2,1)}) custom-call(bf16[64,2048]{1,0:T(8,128)(2,1)} %get-tuple-element.4.token_in, bf16[128,512]{1,0:T(8,128)(2,1)} %get-tuple-element.5.expert_in), custom_call_target="tpu_custom_call" | custom-call | tf_op jit(solution)/shard_map/put_results/pallas_call | solution.py:714

commit v3 on v2

--- a/solution.py
+++ b/solution.py
@@ -11,6 +11,7 @@
 HEAD = 64
 SPAN = 64
 SPANS_AT_ONCE = 2
+STRAIGHT = (("rows", 3), ("hidden", 3))
 NORM_FLOOR = 1.0
 F32 = jnp.float32
 BF = jnp.bfloat16
@@ -176,7 +177,7 @@
     gate_w_in, up_w_in, down_w_in, common_gate_in, common_up_in, common_down_in,
     token_out, expert_out,
     mix, gate_v, out_w, second, rows, meta, gate_up, down, common, common_d,
-    picks, hidden, shared, part, part_in, back, back_in, maps, reads, steps, mixed, mask_v,
+    picks, hidden, shared, part, part_in, back, back_in, pair, chip, reads, steps, mixed, mask_v,
     load_s, zs, zr, ms, mr, rs, rr, hs, hr, cs, cr, ps, pr, fs, fr, os, orr, bs, br, ws, wr,
 ):
     n_z, n_tp, top, cap = sizes
@@ -195,10 +196,22 @@
 
     partner = (e + 1 - 2 * c, t)
 
+    line = n_z == 4
+
+    def z_to(d):
+        if line:
+            return (z, z + 1 - 2 * (z % 2), (z + 2) % 4, 3 - z)[d]
+        return (z + d) % n_z
+
     def z_at(d):
-        return (z + d) % n_z
+        if line:
+            return z_to(d)
+        return (z - d + n_z) % n_z
 
     def z_dev(d):
+        return (z_to(d) * 2 + c, t)
+
+    def back_dev(d):
         return (z_at(d) * 2 + c, t)
 
     def tp_dev(d):
@@ -259,14 +272,14 @@
         return send(rows.at[t, z], rows.at[t, z], zs.at[d], zr.at[d], z_dev(d))
 
     def rows_z_wait(d):
-        w = z_at(n_z - d)
+        w = z_at(d)
         return send(rows.at[t, w], rows.at[t, w], zs.at[d], zr.at[d], z_dev(d))
 
     def meta_z(d):
         return send(meta.at[z], meta.at[z], ms.at[d], mr.at[d], z_dev(d))
 
     def meta_z_wait(d):
-        w = z_at(n_z - d)
+        w = z_at(d)
         return send(meta.at[w], meta.at[w], ms.at[d], mr.at[d], z_dev(d))
 
     for d in range(1, n_z):
@@ -287,19 +300,22 @@
         x_dev, y_dev = (e, x_t), (e, y_t)
 
     class Exchange:
-        def __init__(self, whole, half, sem_s, sem_r):
+        def __init__(self, whole, half, sem_s, sem_r, straight):
             self.whole, self.half, self.sem_s, self.sem_r = whole, half, sem_s, sem_r
+            self.relayed = square and not straight
 
         def copy(self, ref, k, dev):
             return send(ref, ref, self.sem_s(k), self.sem_r(k), dev)
 
         def first(self):
             if square:
-                return [self.copy(self.whole(t), 1, x_dev), self.copy(self.whole(t), 2, y_dev)]
+                near = [self.copy(self.whole(t), 1, x_dev), self.copy(self.whole(t), 2, y_dev)]
+                far = [self.copy(self.whole(t), 3, (e, far_t))]
+                return near + ([] if self.relayed else far)
             return [self.copy(self.whole(t), k, tp_dev(k)) for k in range(1, n_tp)]
 
         def second(self):
-            if square:
+            if self.relayed:
                 return [
                     self.copy(self.half(x_t, 0), 3, y_dev),
                     self.copy(self.half(y_t, 1), 0, x_dev),
@@ -310,17 +326,22 @@
             for copy in self.first():
                 copy.start()
 
+        def near_in(self):
+            return [self.copy(self.whole(x_t), 1, x_dev), self.copy(self.whole(y_t), 2, y_dev)]
+
         def forward(self):
-            if square:
-                ahead = [self.copy(self.whole(x_t), 1, x_dev), self.copy(self.whole(y_t), 2, y_dev)]
-                for came, copy in zip(ahead, self.second()):
+            if self.relayed:
+                for came, copy in zip(self.near_in(), self.second()):
                     came.wait_recv()
                     copy.start()
 
         def finish(self):
-            if square:
+            if self.relayed:
                 self.copy(self.half(far_t, 0), 3, y_dev).wait_recv()
                 self.copy(self.half(far_t, 1), 0, x_dev).wait_recv()
+            elif square:
+                for came in self.near_in() + [self.copy(self.whole(far_t), 3, (e, far_t))]:
+                    came.wait_recv()
             else:
                 for k in range(1, n_tp):
                     src = (t - k + n_tp) % n_tp
@@ -330,11 +351,14 @@
             for copy in self.first() + self.second():
                 copy.wait_send()
 
+    def straight(kind, d):
+        return line and (kind, d) in STRAIGHT
+
     half_rows = row_count // 2
     shared_x = Exchange(
         lambda src: shared.at[src],
         lambda src, i: shared.at[src, pl.ds(i * half_rows, half_rows)],
-        lambda k: cs.at[k], lambda k: cr.at[k],
+        lambda k: cs.at[k], lambda k: cr.at[k], False,
     )
 
     def rows_x(d):
@@ -342,7 +366,7 @@
         return Exchange(
             lambda src: rows.at[src, zz],
             lambda src, i: rows.at[src, zz, pl.ds(i * half_rows, half_rows)],
-            lambda k: rs.at[d, k], lambda k: rr.at[d, k],
+            lambda k: rs.at[d, k], lambda k: rr.at[d, k], straight("rows", d),
         )
 
     def hidden_x(d):
@@ -350,7 +374,7 @@
         return Exchange(
             lambda src: hidden.at[src, zz],
             lambda src, i: hidden.at[src, zz, pl.ds(i * cap, cap)],
-            lambda k: hs.at[d, k], lambda k: hr.at[d, k],
+            lambda k: hs.at[d, k], lambda k: hr.at[d, k], straight("hidden", d),
         )
 
     def each(low, high, step):
@@ -409,7 +433,7 @@
         hidden_x(d).start()
 
     def relay(d):
-        rows_z_wait(n_z - d).wait_recv()
+        rows_z_wait(d).wait_recv()
         rows_x(d).start()
 
     stride = SPANS_AT_ONCE if spans % SPANS_AT_ONCE == 0 else 1
@@ -434,141 +458,176 @@
             steps[0, b, :, lanes] = move
             steps[1, b, :, lanes] = add
 
-    for copy in loads[5:10]:
-        copy.wait()
-    span_step(0)
-    swap_up_in.wait_recv()
-    routed(0)
-    shared_x.forward()
-    loads[11].wait()
-    swap_down.start()
-    each(1, min(3, n_z), relay)
-    for i in range(1, spans // stride):
-        span_step(i)
-    hidden_x(0).forward()
-    rows_x(1).forward()
-    each(3, n_z, relay)
-
     tiles = [pl.ds(g * group, group) for g in range(groups)]
-    mask = mask_v[:lane_tile, :lane_tile]
-    now = [steps[0, 0, :, lanes] for lanes in tiles] + [steps[1, 0, :, lanes] for lanes in tiles]
-    for b in range(1, spans):
-        now = per_heads([steps[0, b, :, lanes] for lanes in tiles] * 2, now, mask, fine=True)
-        for g, lanes in enumerate(tiles):
-            now[groups + g] = now[groups + g] + steps[1, b, :, lanes]
-    for k in range(2 * groups):
-        maps[z, c, :, pl.ds(k * group, group)] = now[k].astype(BF)
-
-    def map_z(d):
-        return send(maps.at[z, c], maps.at[z, c], ps.at[d], pr.at[d], z_dev(d))
-
-    def map_z_wait(d):
-        w = z_at(n_z - d)
-        return send(maps.at[w, c], maps.at[w, c], ps.at[d], pr.at[d], z_dev(d))
-
-    def map_on(d, core):
-        w = z_at(n_z - d)
-        return send(maps.at[w, core], maps.at[w, core], fs.at[d], fr.at[d], partner)
-
-    for d in range(1, n_z):
-        map_z(d).start()
-    map_on(0, c).start()
-
-    def routed_step(d):
-        meta_z_wait(n_z - d).wait_recv()
-        if not isinstance(d, int):
-            pl.when(d > 1)(lambda: rows_x(d).forward())
-        elif d + 1 < n_z:
-            rows_x(d + 1).forward()
-        rows_x(d).finish()
-        routed(d)
-        if isinstance(d, int) and d > 1:
-            hidden_x(d - 1).forward()
-
-    each(1, n_z, routed_step)
-
-    for d in range(1, n_z):
-        map_z_wait(d).wait_recv()
-        map_on(d, c).start()
-    if n_z <= 5:
-        hidden_x(n_z - 1).forward()
-    for d in range(n_z):
-        map_on(d, 1 - c).wait_recv()
-
-    def prefix(i, state):
-        both = maps[i // 2, i % 2]
+    wide = width // 2
+
+    def small_mask():
+        return mask_v[: min(128, wide), : min(128, wide)]
+
+    def compose_own():
         mask = mask_v[:lane_tile, :lane_tile]
-        new = per_heads(
-            [both[:, g * group : (g + 1) * group].astype(F32) for g in range(groups)],
-            state, mask, fine=True,
-        )
-        return [
-            new[g] + both[:, width + g * group : width + (g + 1) * group].astype(F32)
-            for g in range(groups)
-        ]
-
-    state = lax.fori_loop(
-        0, e, prefix, [jnp.zeros((HEAD, group), F32) for _ in range(groups)]
-    )
-
-    loads[10].wait()
-
-    def finish_step(b, state):
-        span = pl.ds(b * SPAN, SPAN)
-        mask, ones = mask_v[:lane_tile, :lane_tile], mask_v[...]
-        many = range(groups)
-        recepts = [mix[0, span, lanes].astype(F32) for lanes in tiles]
-        keys = [mix[1, span, lanes].astype(F32) for lanes in tiles]
-        own = [recepts[g] * keys[g] * self_in[:, tiles[g]] for g in many]
-        both = per_heads(
-            [
-                jnp.concatenate([reads[0, span, lanes], steps[0, b, :, lanes]], axis=0)
-                for lanes in tiles
-            ],
-            state, mask, fine=True,
-        )
-        following = [both[g][SPAN:] + steps[1, b, :, tiles[g]] for g in many]
-        read = [reads[1, span, tiles[g]] + both[g][:SPAN] for g in many]
-        sums = head_sums([jnp.concatenate([read[g], own[g]], axis=0) for g in many], ones)
-        apart = [read[g] - sums[g][:SPAN] * (1.0 / HEAD) for g in many]
-        squares = head_sums([x * x for x in apart], ones)
-        for g, lanes in enumerate(tiles):
-            normed = (
-                apart[g] * lax.rsqrt(squares[g] * (1.0 / HEAD) + NORM_FLOOR) * gain_in[:, lanes]
+        now = [steps[k, 0, :, lanes] for k in range(2) for lanes in tiles]
+        for b in range(1, spans):
+            now = per_heads([steps[0, b, :, lanes] for lanes in tiles] * 2, now, mask, fine=True)
+            for g, lanes in enumerate(tiles):
+                now[groups + g] = now[groups + g] + steps[1, b, :, lanes]
+        for k in range(2):
+            both = now[k * groups : (k + 1) * groups]
+            both = both[0] if groups == 1 else jnp.concatenate(both, axis=1)
+            for h in range(2):
+                pair[c, h, :, k * wide : (k + 1) * wide] = both[
+                    :, h * wide : (h + 1) * wide
+                ].astype(BF)
+
+    def pair_on(core):
+        return send(pair.at[core], pair.at[core], ps.at[0], pr.at[0], partner)
+
+    def chip_z(d, zz):
+        return send(chip.at[zz, c], chip.at[zz, c], ps.at[d], pr.at[d], z_dev(d))
+
+    def chip_on(d, half):
+        zz = z_at(d)
+        return send(chip.at[zz, half], chip.at[zz, half], fs.at[d], fr.at[d], partner)
+
+    def apply(before, now, mask):
+        new = per_heads([now[:, :wide].astype(F32)] * len(before), before, mask, fine=True)
+        new[-1] = new[-1] + now[:, wide:].astype(F32)
+        return new
+
+    def compose_chip():
+        pair_on(1 - c).wait_recv()
+        first = pair[0, c].astype(F32)
+        new = apply([first[:, :wide], first[:, wide:]], pair[1, c], small_mask())
+        for k in range(2):
+            chip[z, c, :, k * wide : (k + 1) * wide] = new[k].astype(BF)
+        for d in range(1, n_z):
+            chip_z(d, z).start()
+
+    def chips_forward():
+        for d in range(1, n_z):
+            chip_z(d, z_at(d)).wait_recv()
+            chip_on(d, c).start()
+
+    def finish_mixer():
+        for d in range(1, n_z):
+            chip_on(d, 1 - c).wait_recv()
+
+        def prefix(i, state):
+            return [apply([state[h]], chip[i, h], small_mask())[0] for h in range(2)]
+
+        state = lax.fori_loop(0, z, prefix, [jnp.zeros((HEAD, wide), F32) for _ in range(2)])
+        behind = [apply([state[h]], pair[0, h], small_mask())[0] for h in range(2)]
+        state = [jnp.where(c == 1, behind[h], state[h]) for h in range(2)]
+        if wide != group:
+            state = jnp.concatenate(state, axis=1)
+            state = [state[:, g * group : (g + 1) * group] for g in range(groups)]
+        loads[10].wait()
+
+        def finish_step(b, state):
+            span = pl.ds(b * SPAN, SPAN)
+            mask, ones = mask_v[:lane_tile, :lane_tile], mask_v[...]
+            many = range(groups)
+            recepts = [mix[0, span, lanes].astype(F32) for lanes in tiles]
+            keys = [mix[1, span, lanes].astype(F32) for lanes in tiles]
+            own = [recepts[g] * keys[g] * self_in[:, tiles[g]] for g in many]
+            both = per_heads(
+                [
+                    jnp.concatenate([reads[0, span, lanes], steps[0, b, :, lanes]], axis=0)
+                    for lanes in tiles
+                ],
+                state, mask, fine=True,
             )
-            out = (normed + sums[g][SPAN:] * mix[2, span, lanes].astype(F32)) * gate_v[
-                span, lanes
-            ].astype(F32)
-            mixed[span, lanes] = out.astype(BF)
-        return following
-
-    lax.fori_loop(0, spans, finish_step, state)
-
-    loads[12].wait()
+            following = [both[g][SPAN:] + steps[1, b, :, tiles[g]] for g in many]
+            read = [reads[1, span, tiles[g]] + both[g][:SPAN] for g in many]
+            sums = head_sums([jnp.concatenate([read[g], own[g]], axis=0) for g in many], ones)
+            apart = [read[g] - sums[g][:SPAN] * (1.0 / HEAD) for g in many]
+            squares = head_sums([x * x for x in apart], ones)
+            for g, lanes in enumerate(tiles):
+                normed = (
+                    apart[g]
+                    * lax.rsqrt(squares[g] * (1.0 / HEAD) + NORM_FLOOR)
+                    * gain_in[:, lanes]
+                )
+                out = (normed + sums[g][SPAN:] * mix[2, span, lanes].astype(F32)) * gate_v[
+                    span, lanes
+                ].astype(F32)
+                mixed[span, lanes] = out.astype(BF)
+            return following
+
+        for b in range(spans):
+            state = finish_step(b, state)
+
     share = positions // n_tp
     wide_cols = min(512, model)
 
-    def project(i, carry):
-        lanes = pl.ds(pl.multiple_of(i * wide_cols, 128), wide_cols)
-        got = dot(mixed[...], out_w[:, lanes]).astype(BF)
-        for k in range(n_tp):
-            part[k, :, lanes] = got[k * share : (k + 1) * share]
-        return carry
-
-    lax.fori_loop(0, model // wide_cols, project, 0)
+    def project():
+        loads[12].wait()
+        for i in range(model // wide_cols):
+            lanes = pl.ds(i * wide_cols, wide_cols)
+            got = dot(mixed[...], out_w[:, lanes]).astype(BF)
+            for k in range(n_tp):
+                part[k, :, lanes] = got[k * share : (k + 1) * share]
 
     def part_to(d):
         return send(
             part.at[(t + d) % n_tp], part_in.at[d], os.at[d], orr.at[d], tp_dev(d)
         )
 
-    for d in range(1, n_tp):
-        part_to(d).start()
-
-    swap_down_in.wait_recv()
+    half_model = model // 2
+
+    def cut(h):
+        return pl.ds(h * half_model, half_model)
+
+    def pair_to(h, j):
+        k = (x_t + 2 * j) % 4 if h == 0 else (y_t + j * (1 - 2 * (t % 2))) % 4
+        dev = x_dev if h == 0 else y_dev
+        i = 2 * h + j
+        return send(part.at[k, :, cut(h)], part_in.at[j, :, cut(h)], os.at[i], orr.at[i], dev)
+
+    def sum_to(h):
+        dev = y_dev if h == 0 else x_dev
+        return send(
+            part_in.at[2, :, cut(h)], part_in.at[3, :, cut(h)], os.at[4 + h], orr.at[4 + h], dev
+        )
+
+    def parts_start():
+        if square:
+            for h in range(2):
+                for j in (1, 0):
+                    pair_to(h, j).start()
+        else:
+            for d in range(1, n_tp):
+                part_to(d).start()
+
+    def parts_turn():
+        for h in range(2):
+            k = y_t if h == 0 else x_t
+            pair_to(h, 1).wait_recv()
+            part_in[2, :, cut(h)] = (
+                part[k, :, cut(h)].astype(F32) + part_in[1, :, cut(h)].astype(F32)
+            ).astype(BF)
+            sum_to(h).start()
+
+    def parts_sum():
+        if square:
+            out = []
+            for h in range(2):
+                pair_to(h, 0).wait_recv()
+                sum_to(h).wait_recv()
+                out.append(
+                    part[t, :, cut(h)].astype(F32)
+                    + part_in[0, :, cut(h)].astype(F32)
+                    + part_in[3, :, cut(h)].astype(F32)
+                )
+            return jnp.concatenate(out, axis=1)
+        summed = part[t].astype(F32)
+        for d in range(1, n_tp):
+            part_to(d).wait_recv()
+            summed = summed + part_in[d].astype(F32)
+        return summed
 
     def back_to(d):
-        return send(back.at[z_at(d)], back_in.at[d], bs.at[d], br.at[d], z_dev(d))
+        return send(back.at[z_at(d)], back_in.at[d], bs.at[d], br.at[d], back_dev(d))
 
     def routed_out(d):
         zz = z_at(d)
@@ -593,25 +652,76 @@
             total = term if total is None else total + term
         return total
 
-    def back_step(d):
-        if not isinstance(d, int):
-            hidden_x(d).forward()
+    def send_back(d):
         back[z_at(d)] = routed_out(d).astype(BF)
         back_to(d).start()
 
-    each(1, n_z, back_step)
+    def other(d):
+        meta_z_wait(d).wait_recv()
+        rows_x(d).finish()
+        routed(d)
+
+    for copy in loads[5:10]:
+        copy.wait()
+    span_step(0)
+    if line:
+        relay(1)
+    swap_up_in.wait_recv()
+    routed(0)
+    shared_x.forward()
+    loads[11].wait()
+    swap_down.start()
+    for i in range(1, spans // stride):
+        span_step(i)
+    if line:
+        rows_x(1).forward()
+    compose_own()
+    pair_on(c).start()
+    if line:
+        relay(2)
+    hidden_x(0).forward()
+    if line:
+        compose_chip()
+        other(1)
+        rows_x(2).forward()
+        relay(3)
+        other(2)
+        hidden_x(1).forward()
+        chips_forward()
+        rows_x(3).forward()
+        hidden_x(2).forward()
+        other(3)
+        hidden_x(3).forward()
+        swap_down_in.wait_recv()
+        send_back(1)
+        send_back(2)
+        finish_mixer()
+        project()
+        parts_start()
+        send_back(3)
+        if square:
+            parts_turn()
+    else:
+        compose_chip()
+        each(1, n_z, relay)
+        each(1, n_z, lambda d: rows_x(d).forward())
+        each(1, n_z, other)
+        each(1, n_z, lambda d: hidden_x(d).forward())
+        swap_down_in.wait_recv()
+        each(1, n_z, send_back)
+        chips_forward()
+        finish_mixer()
+        project()
+        parts_start()
     result = routed_out(0)
-
     loads[13].wait()
     shared_x.finish()
     for k in range(n_tp):
         result = result + dot(shared[k], common_d[pl.ds(k * hid, hid)])
 
-    for d in range(1, n_tp):
-        part_to(d).wait_recv()
-    summed = part[t].astype(F32)
-    for d in range(1, n_tp):
-        summed = summed + part_in[d].astype(F32)
+    if square and not line:
+        parts_turn()
+    summed = parts_sum()
     token_out[...] = summed.astype(BF)
 
     for d in range(1, n_z):
@@ -625,15 +735,22 @@
     for d in range(1, n_z):
         rows_z(d).wait_send()
         meta_z(d).wait_send()
-        map_z(d).wait_send()
+        chip_z(d, z).wait_send()
+        chip_on(d, c).wait_send()
         back_to(d).wait_send()
         rows_x(d).sent()
+    pair_on(c).wait_send()
     for d in range(n_z):
-        map_on(d, c).wait_send()
         hidden_x(d).sent()
     shared_x.sent()
-    for k in range(1, n_tp):
-        part_to(k).wait_send()
+    if square:
+        for h in range(2):
+            sum_to(h).wait_send()
+            for j in range(2):
+                pair_to(h, j).wait_send()
+    else:
+        for k in range(1, n_tp):
+            part_to(k).wait_send()
 
 
 def on_device(n_ep, n_tp, *args):
@@ -685,7 +802,8 @@
             pltpu.VMEM((n_tp, share, model), BF),
             pltpu.VMEM((n_z, row_count, piece), BF),
             pltpu.VMEM((n_z, row_count, piece), BF),
-            pltpu.VMEM((n_z, 2, HEAD, 2 * width), BF),
+            pltpu.VMEM((2, 2, HEAD, width), BF),
+            pltpu.VMEM((n_z, 2, HEAD, width), BF),
             pltpu.VMEM((2, positions, width), F32),
             pltpu.VMEM((2, spans, HEAD, width), F32),
             pltpu.VMEM((positions, width), BF),
@@ -695,7 +813,7 @@
             dma((n_z, n_tp)), dma((n_z, n_tp)), dma((n_z, n_tp)), dma((n_z, n_tp)),
             dma((n_tp,)), dma((n_tp,)),
             dma((n_z,)), dma((n_z,)), dma((n_z,)), dma((n_z,)),
-            dma((n_tp,)), dma((n_tp,)),
+            dma((max(6, n_tp),)), dma((max(6, n_tp),)),
             dma((n_z,)), dma((n_z,)),
             dma((2,)), dma((2,)),
         ],

time: 62.3 us -> 60.3 us (0.968)
  Pallas kernels: 61.3 us -> 59.3 us
    pallas_call x1, Pallas kernels: 59.5 us -> 57.5 us  [on_device(): pl.pallas_call(functools.partial(whole_kernel, (n_z, n_tp, top, cap)), ou...]
where the time goes in v3:
time: 60.3 us; the launch traced here: 60.1 us
  Pallas kernels  59.3 us (98%)
  between operations  0.81 us (1%)
    pallas_call x1, Pallas kernels, on_device(): pl.pallas_call(functools.partial(whole_kernel, (n_z, n_tp, top, cap)), ou...  57.5 us
    pallas_call x1, Pallas kernels, on_device(): pl.pallas_call(put_kernel, out_shape=tuple((jax.ShapeDtypeStruct(x.shape,...  1.74 us

profile of v3, /device:TPU:0, one launch (start us, length us, event | category | flops | bytes accessed | tf_op | source)
XLA Modules:
  0.0 60.1 jit_solution(13387415517315894173)
XLA Ops:
  0.6 57.5 %mixer_and_experts.1 = (bf16[64,2048]{1,0:T(8,128)(2,1)}, bf16[128,512]{1,0:T(8,128)(2,1)}) custom-call(bf16[256,512]{1,0:T(8,128)(2,1)} %recept_in.1, bf16[256,512]{1,0:T(8,128)(2,1)} %keys_in.1, bf16[256,512]{1,0:T(8,128)(2,1)} %values_in.1, bf16[256,512]{1,0:T(8,128)(2,1)} %data_in.1, bf16[256,512]{1,0:T(8,128)(2,1)} %rate_in.1, ...), custom_call_target="tpu_custom_call" | custom-call | tf_op jit(solution)/shard_map/mixer_and_experts/pallas_call | solution.py:779
  58.2 1.7 %put_results.1 = (bf16[64,2048]{1,0:T(8,128)(2,1)}, bf16[128,512]{1,0:T(8,128)(2,1)}) custom-call(bf16[64,2048]{1,0:T(8,128)(2,1)} %get-tuple-element.4.token_in, bf16[128,512]{1,0:T(8,128)(2,1)} %get-tuple-element.5.expert_in), custom_call_target="tpu_custom_call" | custom-call | tf_op jit(solution)/shard_map/put_results/pallas_call | solution.py:832

commit v4 on v3

--- a/solution.py
+++ b/solution.py
@@ -663,11 +663,11 @@
 
     for copy in loads[5:10]:
         copy.wait()
-    span_step(0)
+    swap_up_in.wait_recv()
+    routed(0)
     if line:
         relay(1)
-    swap_up_in.wait_recv()
-    routed(0)
+    span_step(0)
     shared_x.forward()
     loads[11].wait()
     swap_down.start()

time: 60.3 us -> 60 us (level)
  no operation moved by 1% of the time
where the time goes in v4:
time: 60 us; the launch traced here: 59.7 us
  Pallas kernels  58.9 us (98%)
  between operations  0.81 us (1%)
    pallas_call x1, Pallas kernels, on_device(): pl.pallas_call(functools.partial(whole_kernel, (n_z, n_tp, top, cap)), ou...  57.2 us
    pallas_call x1, Pallas kernels, on_device(): pl.pallas_call(put_kernel, out_shape=tuple((jax.ShapeDtypeStruct(x.shape,...  1.74 us

profile of v4, /device:TPU:0, one launch (start us, length us, event | category | flops | bytes accessed | tf_op | source)
XLA Modules:
  0.0 59.7 jit_solution(16953278411644256226)
XLA Ops:
  0.6 57.2 %mixer_and_experts.1 = (bf16[64,2048]{1,0:T(8,128)(2,1)}, bf16[128,512]{1,0:T(8,128)(2,1)}) custom-call(bf16[256,512]{1,0:T(8,128)(2,1)} %recept_in.1, bf16[256,512]{1,0:T(8,128)(2,1)} %keys_in.1, bf16[256,512]{1,0:T(8,128)(2,1)} %values_in.1, bf16[256,512]{1,0:T(8,128)(2,1)} %data_in.1, bf16[256,512]{1,0:T(8,128)(2,1)} %rate_in.1, ...), custom_call_target="tpu_custom_call" | custom-call | tf_op jit(solution)/shard_map/mixer_and_experts/pallas_call | solution.py:779
  57.8 1.7 %put_results.1 = (bf16[64,2048]{1,0:T(8,128)(2,1)}, bf16[128,512]{1,0:T(8,128)(2,1)}) custom-call(bf16[64,2048]{1,0:T(8,128)(2,1)} %get-tuple-element.4.token_in, bf16[128,512]{1,0:T(8,128)(2,1)} %get-tuple-element.5.expert_in), custom_call_target="tpu_custom_call" | custom-call | tf_op jit(solution)/shard_map/put_results/pallas_call | solution.py:832
